TPU v7x, 32 devices: a whole 2x2x4 slice. The times are simulated.
32 devices in a mesh: rep: 2 (over x), fs: 8 (over z, y), tp: 2 (over core).
Axes of the slice: x: 2, y: 2, z: 4, core: 2. Of those that a mesh axis runs over, the one named last changes fastest.
Arguments:
- resid: bfloat16 [12288, 2048], P(('rep', 'fs', 'tp')), may hold values from -6 to 6
- mix_gain: float32 [2048], replicated, may hold values from 0.1 to 1.9
- query_weight: bfloat16 [2048, 1024], P('fs', 'tp'), may hold values from -0.125 to 0.125
- key_weight: bfloat16 [2048, 1024], P('fs', 'tp'), may hold values from -0.125 to 0.125
- value_weight: bfloat16 [2048, 2048], P('fs', 'tp'), may hold values from -0.125 to 0.125
- head_gain: float32 [2048], P('tp'), may hold values from 0.1 to 1.9
- out_weight: bfloat16 [2048, 2048], P('tp', 'fs'), may hold values from -0.125 to 0.125
- mlp_gain: float32 [2048], replicated, may hold values from 0.1 to 1.9
- gate_weight: bfloat16 [2048, 2816], P('fs', 'tp'), may hold values from -0.125 to 0.125
- up_weight: bfloat16 [2048, 2816], P('fs', 'tp'), may hold values from -0.125 to 0.125
- down_weight: bfloat16 [2816, 2048], P('tp', 'fs'), may hold values from -0.109375 to 0.109375
Outputs:
- layer_out: bfloat16 [12288, 2048], P(('rep', 'fs', 'tp'))
All inputs are finite; a program needn't handle non-finite values.
Results may differ from a plain program's by a relative error of at most 0.014.
Values may be sent and summed in bfloat16 or wider, within the bound.
A program may use at most 128 MiB of HBM per device.

v0:
```python
import functools

import jax
import jax.numpy as jnp
from jax import lax
from jax.experimental import pallas as pl
from jax.experimental.pallas import tpu as pltpu
from jax.sharding import PartitionSpec as P

UNITS = 8
MESH = pl.DeviceIdType.MESH


class Exchange:
    def __init__(self, depth, shards, fulls, axes, send_sem, recv_sem):
        self.depth = depth
        self.shards, self.fulls, self.axes = shards, fulls, axes
        self.send_sem, self.recv_sem = send_sem, recv_sem
        self.x = lax.axis_index("rep")
        fs = lax.axis_index("fs")
        self.z = fs // 2
        self.y = lax.rem(fs, 2)

    def barrier(self):
        sem = pltpu.get_barrier_semaphore()
        z, y, x = self.z, self.y, self.x
        pl.semaphore_signal(sem, inc=1, device_id={"rep": 1 - x}, device_id_type=MESH)
        pl.semaphore_signal(sem, inc=1, device_id={"fs": z * 2 + 1 - y}, device_id_type=MESH)

        @pl.when(z > 0)
        def _():
            pl.semaphore_signal(sem, inc=1, device_id={"fs": (z - 1) * 2 + y}, device_id_type=MESH)

        @pl.when(z < self.depth - 1)
        def _():
            pl.semaphore_signal(sem, inc=1, device_id={"fs": (z + 1) * 2 + y}, device_id_type=MESH)

        low = jnp.minimum(z, 1)
        high = jnp.minimum(self.depth - 1 - z, 1)
        pl.semaphore_wait(sem, 2 + low + high)

    def slot(self, w, block, start, count):
        rows, cols = self.shards[w].shape
        if self.axes[w] == 0:
            first = pl.multiple_of(block * rows + start, 16)
            return self.fulls[w].at[pl.ds(first, count), :]
        return self.fulls[w].at[
            pl.ds(pl.multiple_of(start, 16), count), pl.ds(pl.multiple_of(block * cols, 128), cols)
        ]

    def copy(self, w, kind, origin, own=False, incoming=False):
        x, y, z = self.x, self.y, self.z
        unit = self.shards[w].shape[0] // UNITS
        xs = 1 - x if incoming and kind in ("x1", "x2") else x
        start, count = {
            "up": (2 * x, 6), "down": (2 * x, 6), "y": (3 * x, 5), "x1": (6 * xs, 2), "x2": (5 * xs, 3),
        }[kind]
        start, count = start * unit, count * unit
        far = kind == "x2" or (incoming and kind == "y")
        block = origin * 2 + (1 - y if far else y)
        target = {
            "up": {"fs": (z + 1) * 2 + y},
            "down": {"fs": (z - 1) * 2 + y},
            "y": {"fs": z * 2 + 1 - y},
            "x1": {"rep": 1 - x},
            "x2": {"rep": 1 - x},
        }[kind]
        place = self.slot(w, block, start, count)
        source = place
        if own:
            source = self.shards[w].at[pl.ds(pl.multiple_of(start, 16), count), :]
        sends = ("up", "down", "y", "x1", "x2").index(kind)
        receives = (0, 0, 1, 2, 3)[sends]
        return pltpu.make_async_remote_copy(
            src_ref=source,
            dst_ref=place,
            send_sem=self.send_sem.at[w, sends, origin],
            recv_sem=self.recv_sem.at[w, receives, origin],
            device_id=target,
            device_id_type=MESH,
        )

    def each(self, t, body):
        if t == 0:
            body("own", self.z)
            return

        @pl.when(self.z - t >= 0)
        def _():
            body("up", self.z - t)

        @pl.when(self.z + t < self.depth)
        def _():
            body("down", self.z + t)

    def onward(self, w, way, origin, act):
        if way in ("own", "up"):

            @pl.when(self.z < self.depth - 1)
            def _():
                act(self.copy(w, "up", origin, own=way == "own"))

        if way in ("own", "down"):

            @pl.when(self.z > 0)
            def _():
                act(self.copy(w, "down", origin, own=way == "own"))

    def step(self, w, t):
        if t < self.depth:

            def arrive(way, origin):
                if way != "own":
                    self.copy(w, way, origin, incoming=True).wait_recv()
                self.onward(w, way, origin, lambda c: c.start())
                self.copy(w, "y", origin, own=way == "own").start()
                if way != "own":
                    self.copy(w, "x1", origin).start()

            self.each(t, arrive)
        if 1 <= t <= self.depth:

            def cross(way, origin):
                self.copy(w, "y", origin, incoming=True).wait_recv()
                self.copy(w, "x2", origin).start()

            self.each(t - 1, cross)
        if t == self.depth + 1:
            for s in range(self.depth):

                def last(way, origin):
                    if way != "own":
                        self.copy(w, "x1", origin, incoming=True).wait_recv()
                    self.copy(w, "x2", origin, incoming=True).wait_recv()

                self.each(s, last)

    def drain(self, w):
        for s in range(self.depth):

            def sent(way, origin):
                self.onward(w, way, origin, lambda c: c.wait_send())
                self.copy(w, "y", origin, own=way == "own").wait_send()
                if way != "own":
                    self.copy(w, "x1", origin).wait_send()
                self.copy(w, "x2", origin).wait_send()

            self.each(s, sent)


def rotated(v, cosine, sine):
    half = v.shape[-1] // 2
    first, second = v[:, :half], v[:, half:]
    return jnp.concatenate(
        [first * cosine - second * sine, second * cosine + first * sine], axis=-1
    )


def column_dot(left, right, out, width=256):
    @pl.loop(0, out.shape[1] // width)
    def _(c):
        cols = pl.ds(pl.multiple_of(c * width, width), width)
        out[:, cols] = jnp.dot(
            left[...], right[:, cols], preferred_element_type=jnp.float32
        ).astype(out.dtype)


def retain_head(h, heads, tables, proj, memory, head_out):
    cos_ref, sin_ref, inside, query_decay, key_decay, block_decay, gain = tables
    block = inside.shape[-1]
    memory[...] = jnp.zeros_like(memory)
    q_cols = pl.ds(h * DK, DK)
    k_cols = pl.ds((heads + h) * DK, DK)
    v_cols = pl.ds(2 * heads * DK + h * DV, DV)

    @pl.loop(0, proj.shape[0] // block)
    def _(b):
        rows = pl.ds(pl.multiple_of(b * block, block), block)
        cosine, sine = cos_ref[rows, :], sin_ref[rows, :]
        q = rotated(proj[rows, q_cols].astype(jnp.float32), cosine, sine).astype(jnp.bfloat16)
        k = rotated(proj[rows, k_cols].astype(jnp.float32), cosine, sine) * DK ** (-0.5)
        k = k.astype(jnp.bfloat16)
        v = proj[rows, v_cols]
        scores = lax.dot_general(
            q, k, (((1,), (1,)), ((), ())), preferred_element_type=jnp.float32
        )
        weights = (scores * inside[h]).astype(jnp.bfloat16)
        state = memory[...]
        kept = jnp.dot(weights, v, preferred_element_type=jnp.float32) + query_decay[h] * jnp.dot(
            q, state.astype(jnp.bfloat16), preferred_element_type=jnp.float32
        )
        decayed = (k.astype(jnp.float32) * key_decay[h]).astype(jnp.bfloat16)
        memory[...] = state * block_decay[h] + lax.dot_general(
            decayed, v, (((0,), (0,)), ((), ())), preferred_element_type=jnp.float32
        )
        scale = lax.rsqrt(jnp.mean(kept * kept, axis=-1, keepdims=True) + norm_eps)
        head_out[rows, pl.ds(h * DV, DV)] = (
            kept * scale * gain[:, pl.ds(h * DV, DV)]
        ).astype(jnp.bfloat16)


def layer_kernel(depth, axes, *refs):
    count = len(axes)
    shards, refs = refs[:count], refs[count:]
    x_ref, tables, refs = refs[0], refs[1:8], refs[8:]
    fulls, part, refs = refs[:count], refs[count], refs[count + 1 :]
    held, refs = refs[:count], refs[count:]
    mixer, out_w, proj, memory, head_out, send_sem, recv_sem, load_sem, store_sem, fetch_sem = refs
    heads = tables[2].shape[0]
    ex = Exchange(depth, shards, fulls, axes, send_sem, recv_sem)
    loads = [pltpu.make_async_copy(shards[w], held[w], load_sem.at[w]) for w in range(count)]
    for copy in loads:
        copy.start()
    ex.barrier()
    fs = lax.axis_index("fs")
    stores = [
        pltpu.make_async_copy(held[w], ex.slot(w, fs, 0, shards[w].shape[0]), store_sem.at[w])
        for w in range(count)
    ]
    fetch_mixer = pltpu.make_async_copy(fulls[0], mixer, fetch_sem.at[0])
    fetch_out = pltpu.make_async_copy(fulls[1], out_w, fetch_sem.at[1])
    pace = depth - 1
    ready = depth + 1
    for tick in range(pace * (count - 1) + depth + 2):
        for w in range(count):
            t = tick - pace * w
            if 0 <= t <= depth + 1:
                ex.step(w, t)
        if tick == 0:
            for load, store in zip(loads, stores):
                load.wait()
                store.start()
        if tick == 1:
            for copy in stores:
                copy.wait()
        if tick == ready:
            fetch_mixer.start()
        if tick == ready + 1:
            fetch_mixer.wait()
            column_dot(x_ref, mixer, proj)
        for h in range(heads):
            if tick == ready + 2 + h // (heads // 2 if heads > 1 else 1):
                retain_head(h, heads, tables, proj, memory, head_out)
        if tick == pace + ready:
            fetch_out.start()
        if tick == pace + ready + 1:
            fetch_out.wait()
            column_dot(head_out, out_w, part)
    for w in range(count):
        ex.drain(w)


def fits(shards):
    whole = all(s.shape[0] % (UNITS * 16) == 0 and s.shape[1] % 128 == 0 for s in shards)
    return whole and lax.axis_size("rep") == 2 and lax.axis_size("fs") == 8


def layer_start(shards, axes, normed, tables):
    size = lax.axis_size("fs")
    depth = size // 2
    count = len(shards)
    shapes = []
    for s, a in zip(shards, axes):
        shape = list(s.shape)
        shape[a] *= size
        shapes.append(jax.ShapeDtypeStruct(tuple(shape), s.dtype))
    rows = normed.shape[0]
    values = shapes[1].shape[0]
    part = jax.ShapeDtypeStruct((rows, shapes[1].shape[1]), jnp.bfloat16)
    near = pl.BlockSpec(memory_space=pltpu.VMEM)
    far = pl.BlockSpec(memory_space=pl.ANY)
    return pl.pallas_call(
        functools.partial(layer_kernel, depth, tuple(axes)),
        out_shape=shapes + [part],
        in_specs=[far] * count + [near] * (1 + len(tables)),
        out_specs=[far] * count + [near],
        scratch_shapes=[pltpu.VMEM(s.shape, s.dtype) for s in shards]
        + [
            pltpu.VMEM(shapes[0].shape, jnp.bfloat16),
            pltpu.VMEM(shapes[1].shape, jnp.bfloat16),
            pltpu.VMEM((rows, shapes[0].shape[1]), jnp.bfloat16),
            pltpu.VMEM((DK, DV), jnp.float32),
            pltpu.VMEM((rows, values), jnp.bfloat16),
            pltpu.SemaphoreType.DMA((count, 5, depth)),
            pltpu.SemaphoreType.DMA((count, 4, depth)),
            pltpu.SemaphoreType.DMA((count,)),
            pltpu.SemaphoreType.DMA((count,)),
            pltpu.SemaphoreType.DMA((2,)),
        ],
        compiler_params=pltpu.CompilerParams(collective_id=0, has_side_effects=True),
    )(*shards, normed, *tables)


DK = 256
DV = 512
BLOCK = 128


norm_eps = 1e-06
rope_base = 10000.0


def rms_scale(values, gain):
    widened = values.astype(jnp.float32)
    scaled = widened * lax.rsqrt(jnp.mean(widened * widened, axis=-1, keepdims=True) + norm_eps)
    return (scaled * gain).astype(jnp.bfloat16)


def rotation(length_total, half_width):
    position = jnp.arange(length_total, dtype=jnp.float32)
    inverse = 1.0 / rope_base ** jnp.linspace(0.0, 1.0, half_width, dtype=jnp.float32)
    angle = position[:, None] * inverse[None, :]
    return (jnp.cos(angle), jnp.sin(angle))


def rotate(vectors):
    length_total = vectors.shape[0]
    half_width = vectors.shape[-1] // 2
    cosine, sine = rotation(length_total, half_width)
    cosine, sine = cosine[:, None, :], sine[:, None, :]
    first = vectors[..., :half_width]
    second = vectors[..., half_width:]
    return jnp.concatenate(
        [first * cosine - second * sine, second * cosine + first * sine], axis=-1
    )


def decay_tables(head_ids, block):
    log_gamma = jnp.log1p(-(2.0 ** (-5.0 - 2.0 * head_ids.astype(jnp.float32))))
    offset = jnp.arange(block, dtype=jnp.float32)
    distance = offset[:, None] - offset[None, :]
    inside = jnp.where(
        distance >= 0, jnp.exp(log_gamma[:, None, None] * jnp.maximum(distance, 0.0)), 0.0
    )
    query_decay = jnp.exp(log_gamma[:, None] * (offset + 1.0))
    key_decay = jnp.exp(log_gamma[:, None] * (block - 1.0 - offset))
    block_decay = jnp.exp(log_gamma * block)
    return (inside, query_decay, key_decay, block_decay)


def retain(queries, keys, values, head_ids, block):
    length_total, heads, key_width = queries.shape
    value_width = values.shape[-1]
    count = length_total // block
    inside, query_decay, key_decay, block_decay = decay_tables(head_ids, block)

    def blocks(tensor):
        return tensor.reshape(count, block, heads, tensor.shape[-1]).transpose(0, 2, 1, 3)

    def advance(memory, inputs):
        query_tile_rows, key_tile_rows, value_block = inputs
        attention_scores = jnp.einsum(
            "zvf,zjf->zvj", query_tile_rows, key_tile_rows, preferred_element_type=jnp.float32
        )
        weights = (attention_scores * inside).astype(jnp.bfloat16)
        within = jnp.einsum(
            "hlm,hmv->hlv", weights, value_block, preferred_element_type=jnp.float32
        )
        carried = (
            jnp.einsum(
                "hld,hdv->hlv",
                query_tile_rows,
                memory.astype(jnp.bfloat16),
                preferred_element_type=jnp.float32,
            )
            * query_decay[:, :, None]
        )
        weighted_keys = (key_tile_rows.astype(jnp.float32) * key_decay[:, :, None]).astype(
            jnp.bfloat16
        )
        memory = memory * block_decay[:, None, None] + jnp.einsum(
            "hld,hlv->hdv", weighted_keys, value_block, preferred_element_type=jnp.float32
        )
        return (memory, within + carried)

    start_state = jnp.zeros((heads, key_width, value_width), jnp.float32)
    _, outputs = lax.scan(advance, start_state, (blocks(queries), blocks(keys), blocks(values)))
    return outputs.transpose(0, 2, 1, 3).reshape(length_total, heads, value_width)


def head_scale(retained, gain):
    scaled = retained * lax.rsqrt(jnp.mean(retained * retained, axis=-1, keepdims=True) + norm_eps)
    return (scaled.reshape(retained.shape[0], -1) * gain).astype(jnp.bfloat16)


def swap(rows):
    return lax.ppermute(rows, "tp", [(0, 1), (1, 0)])


def join_rows(rows):
    if lax.axis_size("tp") != 2:
        return lax.all_gather(rows, "tp", axis=0, tiled=True)
    first = lax.axis_index("tp") == 0
    got = swap(rows)
    return jnp.concatenate([jnp.where(first, rows, got), jnp.where(first, got, rows)], axis=0)


def share_sum(part):
    if lax.axis_size("tp") != 2:
        summed = lax.psum_scatter(part, "tp", scatter_dimension=0, tiled=True)
        return summed.astype(jnp.float32)
    count = part.shape[0] // 2
    me = lax.axis_index("tp")
    mine = lax.dynamic_slice_in_dim(part, me * count, count, axis=0)
    theirs = lax.dynamic_slice_in_dim(part, (1 - me) * count, count, axis=0)
    return mine.astype(jnp.float32) + swap(theirs).astype(jnp.float32)


def shards(
    resid,
    mix_gain,
    query_weight,
    key_weight,
    value_weight,
    head_gain,
    out_weight,
    mlp_gain,
    gate_weight,
    up_weight,
    down_weight,
):
    token_rows = resid.shape[0]
    length_total = token_rows * lax.axis_size("tp")
    key_cols = query_weight.shape[1]
    heads_here = key_cols // DK
    normed = rms_scale(resid, mix_gain)
    mixer_shard = jnp.concatenate([query_weight, key_weight, value_weight], axis=1)
    mlp_shard = jnp.concatenate([gate_weight, up_weight], axis=1)
    normed_full = join_rows(normed)
    head_ids = lax.axis_index("tp") * heads_here + jnp.arange(heads_here, dtype=jnp.int32)
    pieces = [mixer_shard, out_weight, mlp_shard, down_weight]
    if fits(pieces) and length_total % BLOCK == 0:
        inside, query_decay, key_decay, block_decay = decay_tables(head_ids, BLOCK)
        tables = [
            *rotation(length_total, DK // 2),
            inside,
            query_decay[:, :, None],
            key_decay[:, :, None],
            jnp.broadcast_to(block_decay[:, None, None], (heads_here, DK, 1)),
            head_gain[None, :],
        ]
        _, _, mlp_full, down_full, part = layer_start(pieces, [0, 1, 0, 1], normed_full, tables)
    else:
        mixer_full, out_full, mlp_full, down_full = (
            lax.all_gather(s, "fs", axis=a, tiled=True) for s, a in zip(pieces, [0, 1, 0, 1])
        )
        projected = jnp.dot(
            normed_full, mixer_full, preferred_element_type=jnp.float32
        ).astype(jnp.bfloat16)
        both_keys = projected[:, : 2 * key_cols].astype(jnp.float32)
        both_keys = both_keys.reshape(length_total, 2, heads_here, DK)
        values = projected[:, 2 * key_cols :].reshape(length_total, heads_here, DV)
        query_rot = rotate(both_keys[:, 0]).astype(jnp.bfloat16)
        key_rot = (rotate(both_keys[:, 1]) * DK ** (-0.5)).astype(jnp.bfloat16)
        retained = retain(query_rot, key_rot, values, head_ids, BLOCK)
        head_out = head_scale(retained, head_gain)
        part = jnp.dot(head_out, out_full, preferred_element_type=jnp.float32).astype(jnp.bfloat16)
    mixer_sum = share_sum(part)
    middle = (resid.astype(jnp.float32) + mixer_sum).astype(jnp.bfloat16)
    normed_mlp = rms_scale(middle, mlp_gain)
    local_units = gate_weight.shape[1]
    both = jnp.dot(
        join_rows(normed_mlp),
        mlp_full,
        preferred_element_type=jnp.float32,
    )
    hidden_units = (jax.nn.silu(both[:, :local_units]) * both[:, local_units:]).astype(jnp.bfloat16)
    selected = hidden_units
    mlp_sum = share_sum(
        jnp.dot(selected, down_full, preferred_element_type=jnp.float32).astype(jnp.bfloat16)
    )
    return (middle.astype(jnp.float32) + mlp_sum).astype(jnp.bfloat16)


def solution(mesh):
    placed = (
        P(("rep", "fs", "tp"), None),
        P(),
        P("fs", "tp"),
        P("fs", "tp"),
        P("fs", "tp"),
        P("tp"),
        P("tp", "fs"),
        P(),
        P("fs", "tp"),
        P("fs", "tp"),
        P("tp", "fs"),
    )
    return jax.shard_map(
        shards, mesh=mesh, in_specs=placed, out_specs=P(("rep", "fs", "tp"), None), check_vma=False
    )
```

profile of v0, /device:TPU:0, one launch (start us, length us, event | category | flops | bytes accessed | tf_op | source)
XLA Modules:
  0.0 295.3 jit_solution(8568732003343809043)
XLA Ops:
  0.0 1.8 fusion.1
  1.8 3.0 %fusion.3 = bf16[384,2048]{1,0:T(8,128)(2,1)} fusion(bf16[384,2048]{1,0:T(8,128)(2,1)} %param.11, f32[2048]{0:T(1024)} %param.12, f32[384]{0:T(512)S(1)} %add_rsqrt_fusion.1), kind=kLoop, calls=%fused_computation.11 | loop fusion | flops 3145728 | bytes 3155456 | tf_op jit(solution)/shard_map/convert_element_type | solution.py:306
  4.8 0.5 collective-permute-start
  5.5 0.7 exponential_select_fusion.refs_7_
  6.3 0.8 multiply_exponential_fusion
  7.1 2.2 fusion.15
  9.3 2.2 pad_maximum_fusion.2.refs_0_
  11.6 2.6 pad_maximum_fusion.1.refs_2_
  14.1 1.0 broadcast_select_fusion.3
  15.2 2.0 pad_maximum_fusion.refs_4_
  17.2 0.8 broadcast_in_dim.16.refs_10_
  18.0 236.4 %shard_map.109 = (bf16[2048,2048]{1,0:T(8,128)(2,1)}, bf16[1024,2048]{1,0:T(8,128)(2,1)}, bf16[2048,2816]{1,0:T(8,128)(2,1)}, bf16[1408,2048]{1,0:T(8,128)(2,1)}, bf16[768,2048]{1,0:T(8,128)(2,1)}) custom-call(bf16[256,2048]{1,0:T(8,128)(2,1)} %pad_maximum_fusion.2.refs_0_, bf16[1024,256]{1,0:T(8,128)(2,1)} %refs_1_.1, ...), custom_call_target="tpu_custom_call" | custom-call | tf_op jit(solution)/shard_map/pallas_call | solution.py:272
  254.4 2.7 constant_dynamic-slice_fusion.1
  257.1 3.6 %collective-permute-done.1 = bf16[384,2048]{1,0:T(8,128)(2,1)S(1)} collective-permute-done((bf16[384,2048]{1,0:T(8,128)(2,1)}, bf16[384,2048]{1,0:T(8,128)(2,1)S(1)}, u32[]{:S(2)}, u32[]{:S(2)}) %collective-permute-start.1) | collective-permute-done | bytes 1572896 | tf_op jit(solution)/shard_map/ppermute | solution.py:387
  260.8 2.5 fusion.5
  263.3 0.4 fusion.7
  263.7 0.2 collective-permute-start.2
  263.9 3.3 %collective-permute-done.2 = bf16[384,2048]{1,0:T(8,128)(2,1)S(1)} collective-permute-done((bf16[384,2048]{1,0:T(8,128)(2,1)S(1)}, bf16[384,2048]{1,0:T(8,128)(2,1)S(1)}, u32[]{:S(2)}, u32[]{:S(2)}) %collective-permute-start.2) | collective-permute-done | bytes 1572896 | tf_op jit(solution)/shard_map/ppermute | solution.py:387
  267.2 1.1 broadcast_select_fusion.1
  268.3 12.5 %fusion.9 = f32[768,2816]{1,0:T(8,128)} fusion(bf16[2048,2816]{1,0:T(8,128)(2,1)S(1)} %copy-done.4, bf16[384,2048]{1,0:T(8,128)(2,1)S(1)} %get-tuple-element.14, bf16[384,2048]{1,0:T(8,128)(2,1)S(1)} %get-tuple-element.13), kind=kOutput, calls=%fused_computation.18 | convolution fusion | flops 8864661504 | bytes 23330816 | tf_op jit(solution)/shard_map/dot_general | solution.py:462
  280.8 8.9 %convolution_convert_fusion = bf16[768,2048]{1,0:T(8,128)(2,1)S(1)} fusion(bf16[1408,2048]{1,0:T(8,128)(2,1)S(1)} %bitcast.5, f32[768,2816]{1,0:T(8,128)} %fusion.9), kind=kOutput, calls=%fused_computation.8 | convolution fusion | flops 4437245952 | bytes 17563648 | tf_op jit(solution)/shard_map/dot_general | solution.py:470
  289.8 0.2 collective-permute-start.3
  290.0 3.2 %collective-permute-done.3 = bf16[384,2048]{1,0:T(8,128)(2,1)S(1)} collective-permute-done((bf16[384,2048]{1,0:T(8,128)(2,1)S(1)}, bf16[384,2048]{1,0:T(8,128)(2,1)S(1)}, u32[]{:S(2)}, u32[]{:S(2)}) %collective-permute-start.3) | collective-permute-done | bytes 1572896 | tf_op jit(solution)/shard_map/ppermute | solution.py:387
  293.3 2.0 fusion.8
  (26 shorter events, 0.4 us)
Async XLA Ops:
  0.0 9.3 %copy-start.1 = (bf16[256,512]{1,0:T(8,128)(2,1)S(1)}, bf16[256,512]{1,0:T(8,128)(2,1)}, u32[]{:S(2)}) copy-start(bf16[256,512]{1,0:T(8,128)(2,1)} %param.14) | copy-start | bytes 786436
  4.8 9.3 %collective-permute-start = (bf16[384,2048]{1,0:T(8,128)(2,1)}, bf16[384,2048]{1,0:T(8,128)(2,1)S(1)}, u32[]{:S(2)}, u32[]{:S(2)}) collective-permute-start(bf16[384,2048]{1,0:T(8,128)(2,1)} %fusion.3), channel_id=1, source_target_pairs={{0,1},{1,0},{2,3},{3,2},{4,5},{5,4},{6,7},{7,6},{8,9},{9,8},{10,11... | collective-permute-start | bytes 4718600 | tf_op jit(solution)/shard_map/ppermute | solution.py:387
  5.5 8.6 %copy-start = (bf16[384,2048]{1,0:T(8,128)(2,1)S(1)}, bf16[384,2048]{1,0:T(8,128)(2,1)}, u32[]{:S(2)}) copy-start(bf16[384,2048]{1,0:T(8,128)(2,1)} %param.11) | copy-start | bytes 4718596
  5.5 8.6 %copy-start.2 = (f32[2048]{0:T(1024)S(1)}, f32[2048]{0:T(1024)}, u32[]{:S(2)}) copy-start(f32[2048]{0:T(1024)} %param.12) | copy-start | bytes 24580
  257.1 3.6 %collective-permute-start.1 = (bf16[384,2048]{1,0:T(8,128)(2,1)}, bf16[384,2048]{1,0:T(8,128)(2,1)S(1)}, u32[]{:S(2)}, u32[]{:S(2)}) collective-permute-start(bf16[384,2048]{1,0:T(8,128)(2,1)} %constant_dynamic-slice_fusion.1), channel_id=1, source_target_pairs={{0,1},{1,0},{2,3},{3,2},{4,5},{5,4},{6,7},{7,6},{8,9},{9,8},{10,11... | collective-permute-start | bytes 4718600 | tf_op jit(solution)/shard_map/ppermute | solution.py:387
  257.1 6.1 %copy-start.3 = (f32[2048]{0:T(1024)S(1)}, f32[2048]{0:T(1024)}, u32[]{:S(2)}) copy-start(f32[2048]{0:T(1024)} %param.18) | copy-start | bytes 24580
  260.8 7.5 %copy-start.4 = (bf16[2048,2816]{1,0:T(8,128)(2,1)S(1)}, bf16[2048,2816]{1,0:T(8,128)(2,1)}, u32[]{:S(2)}) copy-start(bf16[2048,2816]{1,0:T(8,128)(2,1)} %get-tuple-element.9) | copy-start | bytes 34603012
  263.7 3.5 %collective-permute-start.2 = (bf16[384,2048]{1,0:T(8,128)(2,1)S(1)}, bf16[384,2048]{1,0:T(8,128)(2,1)S(1)}, u32[]{:S(2)}, u32[]{:S(2)}) collective-permute-start(bf16[384,2048]{1,0:T(8,128)(2,1)S(1)} %fusion.7), channel_id=1, source_target_pairs={{0,1},{1,0},{2,3},{3,2},{4,5},{5,4},{6,7},{7,6},{8,9},{9,8},{10,11... | collective-permute-start | bytes 4718600 | tf_op jit(solution)/shard_map/ppermute | solution.py:387
  267.2 13.6 %slice-start = ((s8[5767168]{0:T(1024)(128)(4,1)}), s8[4194304]{0:T(1024)(128)(4,1)S(1)}, s32[]{:S(2)}) async-start(s8[5767168]{0:T(1024)(128)(4,1)} %bitcast.4), calls=%async_computation | async-start | bytes 8388608
  268.3 12.5 %slice-start.1 = ((s8[5767168]{0:T(1024)(128)(4,1)}), s8[1572864]{0:T(1024)(128)(4,1)S(1)}, s32[]{:S(2)}) async-start(s8[5767168]{0:T(1024)(128)(4,1)} %bitcast.4), calls=%async_computation.1 | async-start | bytes 3145728
  289.8 3.5 %collective-permute-start.3 = (bf16[384,2048]{1,0:T(8,128)(2,1)S(1)}, bf16[384,2048]{1,0:T(8,128)(2,1)S(1)}, u32[]{:S(2)}, u32[]{:S(2)}) collective-permute-start(bf16[384,2048]{1,0:T(8,128)(2,1)S(1)} %constant_dynamic-slice_fusion), channel_id=1, source_target_pairs={{0,1},{1,0},{2,3},{3,2},{4,5},{5,4},{6,7},{7,6},{8,9},{9,8},{10,11... | collective-permute-start | bytes 4718600 | tf_op jit(solution)/shard_map/ppermute | solution.py:387
where the time goes:
time: 296 us; the launch traced here: 295 us
  Pallas kernels  236 us (80%)
  other arithmetic  22.6 us (8%)
  matrix products  21.3 us (7%)
  waiting for transfers between devices  10.1 us (3%)
  local copies, waits for them, and re-layouts  3.73 us (1%)
    pallas_call x1, Pallas kernels, layer_start(): pl.pallas_call(functools.partial(layer_kernel, depth, tuple(axes)), out_s...  236 us
    dot_general x1, matrix products, shards(): jnp.dot(join_rows(normed_mlp), mlp_full, preferred_element_type=jnp.float32)  12.5 us
    ppermute x4, waiting for transfers between devices, swap(): return lax.ppermute(rows, 'tp', [(0, 1), (1, 0)])  10.1 us
    dot_general x1, matrix products, shards(): jnp.dot(selected, down_full, preferred_element_type=jnp.float32)  8.86 us
  transfers between devices with their start and end apart: 4, of which 3 were waited for; matrix products, arithmetic and copies ran while one was open for 3% of the time, Pallas kernels for 0%

commit v1 on v0

v1 whole, which is shorter than its diff:
```python
import functools
import math

import jax
import jax.numpy as jnp
import numpy as np
from jax import lax
from jax.experimental import pallas as pl
from jax.experimental.pallas import tpu as pltpu
from jax.sharding import PartitionSpec as P

UNITS = 8
MESH = pl.DeviceIdType.MESH


class Stream:
    def __init__(self, w, first, count, along_z, along_y):
        self.w, self.first, self.count = w, first, count
        self.along_z, self.along_y = along_z, along_y


class Exchange:
    def __init__(self, depth, streams, shapes, axes, fulls, send_sem, recv_sem):
        self.depth, self.streams = depth, streams
        self.shapes, self.axes, self.fulls = shapes, axes, fulls
        self.send_sem, self.recv_sem = send_sem, recv_sem
        self.x = lax.axis_index("rep")
        fs = lax.axis_index("fs")
        self.z = fs // 2
        self.y = lax.rem(fs, 2)

    def barrier(self):
        sem = pltpu.get_barrier_semaphore()
        z, y, x = self.z, self.y, self.x
        core = lax.axis_index("tp")
        pl.semaphore_signal(sem, inc=1, device_id={"tp": 1 - core}, device_id_type=MESH)
        pl.semaphore_signal(sem, inc=1, device_id={"rep": 1 - x}, device_id_type=MESH)
        pl.semaphore_signal(sem, inc=1, device_id={"fs": z * 2 + 1 - y}, device_id_type=MESH)

        @pl.when(z > 0)
        def _():
            pl.semaphore_signal(sem, inc=1, device_id={"fs": (z - 1) * 2 + y}, device_id_type=MESH)

        @pl.when(z < self.depth - 1)
        def _():
            pl.semaphore_signal(sem, inc=1, device_id={"fs": (z + 1) * 2 + y}, device_id_type=MESH)

        low = jnp.minimum(z, 1)
        high = jnp.minimum(self.depth - 1 - z, 1)
        pl.semaphore_wait(sem, 3 + low + high)

    def slot(self, w, block, start, count):
        rows, cols = self.shapes[w]
        if self.axes[w] == 0:
            first = pl.multiple_of(block * rows + start, 16)
            return self.fulls[w].at[pl.ds(first, count), :]
        return self.fulls[w].at[
            pl.ds(pl.multiple_of(start, 16), count), pl.ds(pl.multiple_of(block * cols, 128), cols)
        ]

    def copy(self, s, kind, origin, incoming=False):
        stream = self.streams[s]
        x, y, z = self.x, self.y, self.z
        a, b = stream.along_z, stream.along_y
        unit = stream.count // UNITS
        xs = 1 - x if incoming and kind in ("x1", "x2") else x
        start, count = {
            "up": ((UNITS - a) * x, a),
            "down": ((UNITS - a) * x, a),
            "y": ((UNITS - b) * x, b),
            "x1": (a * xs, UNITS - a),
            "x2": (b * xs, UNITS - b),
        }[kind]
        start, count = stream.first + start * unit, count * unit
        far = kind == "x2" or (incoming and kind == "y")
        block = origin * 2 + (1 - y if far else y)
        target = {
            "up": {"fs": (z + 1) * 2 + y},
            "down": {"fs": (z - 1) * 2 + y},
            "y": {"fs": z * 2 + 1 - y},
            "x1": {"rep": 1 - x},
            "x2": {"rep": 1 - x},
        }[kind]
        place = self.slot(stream.w, block, start, count)
        sends = ("up", "down", "y", "x1", "x2").index(kind)
        receives = (0, 0, 1, 2, 3)[sends]
        return pltpu.make_async_remote_copy(
            src_ref=place,
            dst_ref=place,
            send_sem=self.send_sem.at[s, sends, origin],
            recv_sem=self.recv_sem.at[s, receives, origin],
            device_id=target,
            device_id_type=MESH,
        )

    def each(self, t, body):
        if t == 0:
            body("own", self.z)
            return

        @pl.when(self.z - t >= 0)
        def _():
            body("up", self.z - t)

        @pl.when(self.z + t < self.depth)
        def _():
            body("down", self.z + t)

    def onward(self, s, way, origin, act):
        if way in ("own", "up"):

            @pl.when(self.z < self.depth - 1)
            def _():
                act(self.copy(s, "up", origin))

        if way in ("own", "down"):

            @pl.when(self.z > 0)
            def _():
                act(self.copy(s, "down", origin))

    def step(self, s, t):
        if t < self.depth:

            def arrive(way, origin):
                if way != "own":
                    self.copy(s, way, origin, incoming=True).wait_recv()
                self.onward(s, way, origin, lambda c: c.start())
                self.copy(s, "y", origin).start()
                if way != "own":
                    self.copy(s, "x1", origin).start()

            self.each(t, arrive)
        if 1 <= t <= self.depth:

            def cross(way, origin):
                self.copy(s, "y", origin, incoming=True).wait_recv()
                self.copy(s, "x2", origin).start()

            self.each(t - 1, cross)
        if t == self.depth + 1:
            for back in range(self.depth):

                def last(way, origin):
                    if way != "own":
                        self.copy(s, "x1", origin, incoming=True).wait_recv()
                    self.copy(s, "x2", origin, incoming=True).wait_recv()

                self.each(back, last)

    def drain(self, s):
        for back in range(self.depth):

            def sent(way, origin):
                self.onward(s, way, origin, lambda c: c.wait_send())
                self.copy(s, "y", origin).wait_send()
                if way != "own":
                    self.copy(s, "x1", origin).wait_send()
                self.copy(s, "x2", origin).wait_send()

            self.each(back, sent)


class Peer:
    def __init__(self, send_sem, recv_sem):
        self.send_sem, self.recv_sem = send_sem, recv_sem
        self.core = lax.axis_index("tp")

    def copy(self, index, source, place):
        return pltpu.make_async_remote_copy(
            src_ref=source,
            dst_ref=place,
            send_sem=self.send_sem.at[index],
            recv_sem=self.recv_sem.at[index],
            device_id={"tp": 1 - self.core},
            device_id_type=MESH,
        )


def rotated(v, cosine, sine):
    half = v.shape[-1] // 2
    first, second = v[:, :half], v[:, half:]
    return jnp.concatenate(
        [first * cosine - second * sine, second * cosine + first * sine], axis=-1
    )


def column_dot(left, right, out, first, last, width=256):
    @pl.loop(first, last)
    def _(c):
        cols = pl.ds(pl.multiple_of(c * width, width), width)
        out[:, cols] = jnp.dot(
            left[...], right[:, cols], preferred_element_type=jnp.float32
        ).astype(out.dtype)


def scaled_rows(values, gain):
    scale = lax.rsqrt(jnp.mean(values * values, axis=-1, keepdims=True) + norm_eps)
    return (values * scale * gain).astype(jnp.bfloat16)


def decay_rates(ids):
    return [math.log1p(-(2.0 ** (-5.0 - 2.0 * i))) for i in ids]


def make_tables(heads, inside, query_decay, key_decay):
    core = lax.axis_index("tp")
    block = inside.shape[-1]
    rates = decay_rates(range(2 * heads))
    row = lax.broadcasted_iota(jnp.int32, (block, block), 0).astype(jnp.float32)
    col = lax.broadcasted_iota(jnp.int32, (block, block), 1).astype(jnp.float32)
    distance = row - col
    for h in range(heads):
        rate = jnp.where(core == 0, rates[h], rates[heads + h])
        inside[h] = jnp.where(
            distance >= 0, jnp.exp(rate * jnp.maximum(distance, 0.0)), 0.0
        )
        query_decay[h] = jnp.exp(rate * (row + 1.0))
        key_decay[h] = jnp.exp(rate * (block - 1.0 - row))


def retain_blocks(h, heads, first, last, tables, proj, memory, head_out):
    cos_ref, sin_ref, inside, query_decay, key_decay, gain = tables
    core = lax.axis_index("tp")
    block = inside.shape[-1]
    rates = decay_rates(range(2 * heads))
    block_decay = jnp.where(
        core == 0, math.exp(rates[h] * block), math.exp(rates[heads + h] * block)
    )
    if first == 0:
        memory[...] = jnp.zeros_like(memory)
    q_cols = pl.ds(h * DK, DK)
    k_cols = pl.ds((heads + h) * DK, DK)
    v_cols = pl.ds(2 * heads * DK + h * DV, DV)

    @pl.loop(first, last)
    def _(b):
        rows = pl.ds(pl.multiple_of(b * block, block), block)
        cosine, sine = cos_ref[rows, :], sin_ref[rows, :]
        q = rotated(proj[rows, q_cols].astype(jnp.float32), cosine, sine).astype(jnp.bfloat16)
        k = rotated(proj[rows, k_cols].astype(jnp.float32), cosine, sine) * DK ** (-0.5)
        k = k.astype(jnp.bfloat16)
        v = proj[rows, v_cols]
        scores = lax.dot_general(
            q, k, (((1,), (1,)), ((), ())), preferred_element_type=jnp.float32
        )
        weights = (scores * inside[h]).astype(jnp.bfloat16)
        state = memory[...]
        kept = jnp.dot(weights, v, preferred_element_type=jnp.float32) + query_decay[h][
            :, 0:1
        ] * jnp.dot(q, state.astype(jnp.bfloat16), preferred_element_type=jnp.float32)
        decayed = (k.astype(jnp.float32) * key_decay[h][:, 0:1]).astype(jnp.bfloat16)
        memory[...] = state * block_decay + lax.dot_general(
            decayed, v, (((0,), (0,)), ((), ())), preferred_element_type=jnp.float32
        )
        scale = lax.rsqrt(jnp.mean(kept * kept, axis=-1, keepdims=True) + norm_eps)
        head_out[rows, pl.ds(h * DV, DV)] = (
            kept * scale * gain[:, pl.ds(h * DV, DV)]
        ).astype(jnp.bfloat16)


ROWS = 64
WIDE = 512


def layer_kernel(depth, streams, shapes, heads, *refs):
    args, refs = refs[:13], refs[13:]
    resid, mix_gain, query, key, value, head_gain, out_w, mlp_gain, gate, up, down, cos, sin = args
    out, refs = refs[0], refs[1:]
    fulls, refs = refs[:4], refs[4:]
    mixer, out_full, mlp, down_full = fulls
    held, refs = refs[:6], refs[6:]
    x, gain_mix, gain_head, gain_mlp, cos_v, sin_v = held
    normed, both, proj, memory, head_out, hidden, part, sent, got, middle, result, refs = (
        *refs[:11],
        refs[11:],
    )
    inside, query_decay, key_decay, refs = *refs[:3], refs[3:]
    send_sem, recv_sem, load_sem, peer_send, peer_recv, out_sem = refs
    ex = Exchange(depth, streams, shapes, (0, 1, 0, 1), fulls, send_sem, recv_sem)
    peer = Peer(peer_send, peer_recv)
    core = lax.axis_index("tp")
    fs = lax.axis_index("fs")
    rows = x.shape[0]
    qc, kc, vc = query.shape[1], key.shape[1], value.shape[1]
    units = gate.shape[1]

    mixer_own = pl.ds(pl.multiple_of(fs * shapes[0][0], 16), shapes[0][0])
    mlp_own = pl.ds(pl.multiple_of(fs * shapes[2][0], 16), shapes[2][0])
    pairs = [
        (query, mixer.at[mixer_own, pl.ds(0, qc)]),
        (key, mixer.at[mixer_own, pl.ds(qc, kc)]),
        (value, mixer.at[mixer_own, pl.ds(qc + kc, vc)]),
        (out_w, ex.slot(1, fs, 0, shapes[1][0])),
        (resid, x),
        (mix_gain, gain_mix),
        (down, ex.slot(3, fs, 0, shapes[3][0])),
        (cos, cos_v),
        (sin, sin_v),
        (head_gain, gain_head),
        (mlp_gain, gain_mlp),
    ]
    loads = [
        pltpu.make_async_copy(source, place, load_sem.at[i])
        for i, (source, place) in enumerate(pairs)
    ]
    for load in loads[:6]:
        load.start()

    @pl.loop(0, units // 128)
    def _(j):
        cols = pl.ds(pl.multiple_of(j * 128, 128), 128)
        for i, source in enumerate((gate, up)):
            place = pl.ds(pl.multiple_of(j * 256, 128) + i * 128, 128)
            pltpu.make_async_copy(
                source.at[:, cols], mlp.at[mlp_own, place], load_sem.at[len(pairs)]
            ).start()

    for load in loads[6:]:
        load.start()
    mlp_slot = ex.slot(2, fs, 0, shapes[2][0])
    mlp_load = pltpu.make_async_copy(mlp_slot, mlp_slot, load_sem.at[len(pairs)])

    ex.barrier()

    own = pl.ds(pl.multiple_of(core * rows, 16), rows)
    other = pl.ds(pl.multiple_of((1 - core) * rows, 16), rows)
    join_mix = peer.copy(0, normed.at[own, :], normed.at[own, :])
    join_mlp = peer.copy(1, both.at[own, :], both.at[own, :])

    def norm_mix():
        loads[4].wait()
        loads[5].wait()

        @pl.loop(0, rows // ROWS)
        def _(r):
            here = pl.ds(pl.multiple_of(r * ROWS, ROWS), ROWS)
            there = pl.ds(pl.multiple_of(core * rows + r * ROWS, ROWS), ROWS)
            normed[there, :] = scaled_rows(x[here, :].astype(jnp.float32), gain_mix[...])

        join_mix.start()
        make_tables(heads, inside, query_decay, key_decay)
        for load in loads[7:]:
            load.wait()

    def share(index, c):
        cols = pl.ds(c * WIDE, WIDE)
        return peer.copy(index + c, sent.at[:, cols], got.at[:, cols])

    chunks = part.shape[1] // WIDE

    def product(left, right, index):
        for c in range(chunks):

            @pl.loop(0, WIDE // 256)
            def _(i):
                cols = pl.ds(pl.multiple_of(c * WIDE + i * 256, 256), 256)
                sent[:, cols] = jnp.dot(
                    left[other, :], right[:, cols], preferred_element_type=jnp.float32
                ).astype(jnp.bfloat16)

            share(index, c).start()
        for c in range(chunks):

            @pl.loop(0, WIDE // 256)
            def _(i):
                cols = pl.ds(pl.multiple_of(c * WIDE + i * 256, 256), 256)
                part[:, cols] = jnp.dot(
                    left[own, :], right[:, cols], preferred_element_type=jnp.float32
                ).astype(jnp.bfloat16)

    def norm_mlp():
        for c in range(chunks):
            share(2, c).wait()

        @pl.loop(0, rows // ROWS)
        def _(r):
            here = pl.ds(pl.multiple_of(r * ROWS, ROWS), ROWS)
            there = pl.ds(pl.multiple_of(core * rows + r * ROWS, ROWS), ROWS)
            total = part[here, :].astype(jnp.float32) + got[here, :].astype(jnp.float32)
            mid = (x[here, :].astype(jnp.float32) + total).astype(jnp.bfloat16)
            middle[here, :] = mid
            both[there, :] = scaled_rows(mid.astype(jnp.float32), gain_mlp[...])

        join_mlp.start()

    def expand():
        @pl.loop(0, units // 128)
        def _(j):
            cols = pl.ds(pl.multiple_of(j * 256, 256), 256)
            pair = jnp.dot(both[...], mlp[:, cols], preferred_element_type=jnp.float32)
            place = pl.ds(pl.multiple_of(j * 128, 128), 128)
            hidden[:, place] = (jax.nn.silu(pair[:, :128]) * pair[:, 128:]).astype(jnp.bfloat16)

    def finish():
        writes = []
        for c in range(chunks):
            cols = pl.ds(c * WIDE, WIDE)
            share(2 + chunks, c).wait()
            total = part[:, cols].astype(jnp.float32) + got2(cols)
            result[:, cols] = (middle[:, cols].astype(jnp.float32) + total).astype(jnp.bfloat16)
            write = pltpu.make_async_copy(result.at[:, cols], out.at[:, cols], out_sem.at[c])
            write.start()
            writes.append(write)
        for write in writes:
            write.wait()

    def got2(cols):
        return got[:, cols].astype(jnp.float32)

    blocks = proj.shape[0] // inside.shape[-1]
    tables = (cos_v, sin_v, inside, query_decay, key_decay, gain_head)
    columns = proj.shape[1] // 256
    plan = {0: [norm_mix]}
    span = 2 * (depth + 2) - 6
    half = blocks // 2
    first = 2 * (depth + 1) + 1

    def project(low, high):
        if low == 0:
            join_mix.wait()
        column_dot(normed, mixer, proj, low, high)

    plan[first] = [lambda: project(0, columns // 2)]
    plan[first + 1] = [lambda: project(columns // 2, columns)]
    at = first + 2
    for h in range(heads):
        for low, high in ((0, half), (half, blocks)):
            plan.setdefault(at, []).append(
                functools.partial(
                    retain_blocks, h, heads, low, high, tables, proj, memory, head_out
                )
            )
            at += 1
    plan.setdefault(first + 6, []).append(lambda: product(head_out, out_full, 2))
    plan.setdefault(first + 7, []).append(norm_mlp)

    def mlp_in():
        join_mlp.wait()
        expand()

    plan.setdefault(first + 12, []).append(mlp_in)
    plan.setdefault(first + 18, []).append(lambda: product(hidden, down_full, 2 + chunks))
    plan[first + 18].append(finish)
    count = len(streams)
    begin = {0: loads[:3], 2: loads[3:4], 4: [mlp_load], 6: loads[6:7]}
    for tick in range(first + 19):
        for s in range(count):
            t, odd = divmod(tick - 6 * (s // 2), 2)
            if odd == s % 2 and 0 <= t <= depth + 1:
                if t == 0:
                    for load in begin.get(s, ()):
                        load.wait()
                ex.step(s, t)
        for job in plan.get(tick, ()):
            job()
    for s in range(count):
        ex.drain(s)


def cut(total):
    whole = total // (UNITS * 16)
    first = (whole + 1) // 2 * UNITS * 16
    return first, total - first


def plan_streams(shapes):
    streams = []
    for w, (rows, _) in enumerate(shapes):
        first, second = cut(rows)
        streams.append(Stream(w, 0, first, 6, 5))
        streams.append(Stream(w, first, second, 7, 4))
    return streams


def rotation_tables(length_total, half_width):
    position = np.arange(length_total, dtype=np.float32)
    inverse = (1.0 / rope_base ** np.linspace(0.0, 1.0, half_width)).astype(np.float32)
    angle = (position[:, None] * inverse[None, :]).astype(np.float64)
    return np.cos(angle).astype(np.float32), np.sin(angle).astype(np.float32)


def fits(shapes, rows, heads):
    whole = all(r % (UNITS * 16) == 0 and r >= 2 * UNITS * 16 and c % 128 == 0 for r, c in shapes)
    sizes = lax.axis_size("rep") == 2 and lax.axis_size("fs") == 8 and lax.axis_size("tp") == 2
    return whole and sizes and rows % BLOCK == 0 and heads == 2


def layer(args, shapes, heads):
    resid, query, key, value, gate = args[0], args[2], args[3], args[4], args[8]
    size = lax.axis_size("fs")
    depth = size // 2
    rows, width = resid.shape
    length_total = 2 * rows
    streams = plan_streams(shapes)
    count = len(streams)
    fulls = []
    for (r, c), axis in zip(shapes, (0, 1, 0, 1)):
        fulls.append((r * size, c) if axis == 0 else (r, c * size))
    cosine, sine = rotation_tables(length_total, DK // 2)
    far = pl.BlockSpec(memory_space=pl.ANY)
    bf, f32 = jnp.bfloat16, jnp.float32
    vm = pltpu.VMEM
    dma = pltpu.SemaphoreType.DMA
    chunks = width // WIDE
    args = [a[None, :] if a.ndim == 1 else a for a in args]
    return pl.pallas_call(
        functools.partial(layer_kernel, depth, streams, shapes, heads),
        out_shape=jax.ShapeDtypeStruct((rows, width), bf),
        in_specs=[far] * 13,
        out_specs=far,
        scratch_shapes=[vm(s, bf) for s in fulls]
        + [
            vm((rows, width), bf),
            vm(args[1].shape, f32),
            vm(args[5].shape, f32),
            vm(args[7].shape, f32),
            vm(cosine.shape, f32),
            vm(sine.shape, f32),
            vm((length_total, width), bf),
            vm((length_total, width), bf),
            vm((length_total, shapes[0][1]), bf),
            vm((DK, DV), f32),
            vm((length_total, heads * DV), bf),
            vm((length_total, gate.shape[1]), bf),
            vm((rows, width), bf),
            vm((rows, width), bf),
            vm((rows, width), bf),
            vm((rows, width), bf),
            vm((rows, width), bf),
            vm((heads, BLOCK, BLOCK), f32),
            vm((heads, BLOCK, BLOCK), f32),
            vm((heads, BLOCK, BLOCK), f32),
            dma((count, 5, depth)),
            dma((count, 4, depth)),
            dma((12,)),
            dma((2 + 2 * chunks,)),
            dma((2 + 2 * chunks,)),
            dma((chunks,)),
        ],
        compiler_params=pltpu.CompilerParams(
            collective_id=0, has_side_effects=True, vmem_limit_bytes=67043328
        ),
    )(*args, jnp.asarray(cosine), jnp.asarray(sine))


DK = 256
DV = 512
BLOCK = 128


norm_eps = 1e-06
rope_base = 10000.0


def rms_scale(values, gain):
    widened = values.astype(jnp.float32)
    scaled = widened * lax.rsqrt(jnp.mean(widened * widened, axis=-1, keepdims=True) + norm_eps)
    return (scaled * gain).astype(jnp.bfloat16)


def rotation(length_total, half_width):
    position = jnp.arange(length_total, dtype=jnp.float32)
    inverse = 1.0 / rope_base ** jnp.linspace(0.0, 1.0, half_width, dtype=jnp.float32)
    angle = position[:, None] * inverse[None, :]
    return (jnp.cos(angle), jnp.sin(angle))


def rotate(vectors):
    length_total = vectors.shape[0]
    half_width = vectors.shape[-1] // 2
    cosine, sine = rotation(length_total, half_width)
    cosine, sine = cosine[:, None, :], sine[:, None, :]
    first = vectors[..., :half_width]
    second = vectors[..., half_width:]
    return jnp.concatenate(
        [first * cosine - second * sine, second * cosine + first * sine], axis=-1
    )


def decay_tables(head_ids, block):
    log_gamma = jnp.log1p(-(2.0 ** (-5.0 - 2.0 * head_ids.astype(jnp.float32))))
    offset = jnp.arange(block, dtype=jnp.float32)
    distance = offset[:, None] - offset[None, :]
    inside = jnp.where(
        distance >= 0, jnp.exp(log_gamma[:, None, None] * jnp.maximum(distance, 0.0)), 0.0
    )
    query_decay = jnp.exp(log_gamma[:, None] * (offset + 1.0))
    key_decay = jnp.exp(log_gamma[:, None] * (block - 1.0 - offset))
    block_decay = jnp.exp(log_gamma * block)
    return (inside, query_decay, key_decay, block_decay)


def retain(queries, keys, values, head_ids, block):
    length_total, heads, key_width = queries.shape
    value_width = values.shape[-1]
    count = length_total // block
    inside, query_decay, key_decay, block_decay = decay_tables(head_ids, block)

    def blocks(tensor):
        return tensor.reshape(count, block, heads, tensor.shape[-1]).transpose(0, 2, 1, 3)

    def advance(memory, inputs):
        query_tile_rows, key_tile_rows, value_block = inputs
        attention_scores = jnp.einsum(
            "zvf,zjf->zvj", query_tile_rows, key_tile_rows, preferred_element_type=jnp.float32
        )
        weights = (attention_scores * inside).astype(jnp.bfloat16)
        within = jnp.einsum(
            "hlm,hmv->hlv", weights, value_block, preferred_element_type=jnp.float32
        )
        carried = (
            jnp.einsum(
                "hld,hdv->hlv",
                query_tile_rows,
                memory.astype(jnp.bfloat16),
                preferred_element_type=jnp.float32,
            )
            * query_decay[:, :, None]
        )
        weighted_keys = (key_tile_rows.astype(jnp.float32) * key_decay[:, :, None]).astype(
            jnp.bfloat16
        )
        memory = memory * block_decay[:, None, None] + jnp.einsum(
            "hld,hlv->hdv", weighted_keys, value_block, preferred_element_type=jnp.float32
        )
        return (memory, within + carried)

    start_state = jnp.zeros((heads, key_width, value_width), jnp.float32)
    _, outputs = lax.scan(advance, start_state, (blocks(queries), blocks(keys), blocks(values)))
    return outputs.transpose(0, 2, 1, 3).reshape(length_total, heads, value_width)


def head_scale(retained, gain):
    scaled = retained * lax.rsqrt(jnp.mean(retained * retained, axis=-1, keepdims=True) + norm_eps)
    return (scaled.reshape(retained.shape[0], -1) * gain).astype(jnp.bfloat16)


def swap(rows):
    return lax.ppermute(rows, "tp", [(0, 1), (1, 0)])


def join_rows(rows):
    if lax.axis_size("tp") != 2:
        return lax.all_gather(rows, "tp", axis=0, tiled=True)
    first = lax.axis_index("tp") == 0
    got = swap(rows)
    return jnp.concatenate([jnp.where(first, rows, got), jnp.where(first, got, rows)], axis=0)


def share_sum(part):
    if lax.axis_size("tp") != 2:
        summed = lax.psum_scatter(part, "tp", scatter_dimension=0, tiled=True)
        return summed.astype(jnp.float32)
    count = part.shape[0] // 2
    me = lax.axis_index("tp")
    mine = lax.dynamic_slice_in_dim(part, me * count, count, axis=0)
    theirs = lax.dynamic_slice_in_dim(part, (1 - me) * count, count, axis=0)
    return mine.astype(jnp.float32) + swap(theirs).astype(jnp.float32)


def shards(
    resid,
    mix_gain,
    query_weight,
    key_weight,
    value_weight,
    head_gain,
    out_weight,
    mlp_gain,
    gate_weight,
    up_weight,
    down_weight,
):
    token_rows = resid.shape[0]
    length_total = token_rows * lax.axis_size("tp")
    key_cols = query_weight.shape[1]
    heads_here = key_cols // DK
    shapes = [
        (query_weight.shape[0], query_weight.shape[1] + key_weight.shape[1] + value_weight.shape[1]),
        out_weight.shape,
        (gate_weight.shape[0], gate_weight.shape[1] + up_weight.shape[1]),
        down_weight.shape,
    ]
    if fits(shapes, token_rows, heads_here):
        args = [
            resid, mix_gain, query_weight, key_weight, value_weight, head_gain,
            out_weight, mlp_gain, gate_weight, up_weight, down_weight,
        ]
        return layer(args, shapes, heads_here)
    normed = rms_scale(resid, mix_gain)
    mixer_shard = jnp.concatenate([query_weight, key_weight, value_weight], axis=1)
    mlp_shard = jnp.concatenate([gate_weight, up_weight], axis=1)
    normed_full = join_rows(normed)
    head_ids = lax.axis_index("tp") * heads_here + jnp.arange(heads_here, dtype=jnp.int32)
    pieces = [mixer_shard, out_weight, mlp_shard, down_weight]
    mixer_full, out_full, mlp_full, down_full = (
        lax.all_gather(s, "fs", axis=a, tiled=True) for s, a in zip(pieces, [0, 1, 0, 1])
    )
    projected = jnp.dot(
        normed_full, mixer_full, preferred_element_type=jnp.float32
    ).astype(jnp.bfloat16)
    both_keys = projected[:, : 2 * key_cols].astype(jnp.float32)
    both_keys = both_keys.reshape(length_total, 2, heads_here, DK)
    values = projected[:, 2 * key_cols :].reshape(length_total, heads_here, DV)
    query_rot = rotate(both_keys[:, 0]).astype(jnp.bfloat16)
    key_rot = (rotate(both_keys[:, 1]) * DK ** (-0.5)).astype(jnp.bfloat16)
    retained = retain(query_rot, key_rot, values, head_ids, BLOCK)
    head_out = head_scale(retained, head_gain)
    part = jnp.dot(head_out, out_full, preferred_element_type=jnp.float32).astype(jnp.bfloat16)
    mixer_sum = share_sum(part)
    middle = (resid.astype(jnp.float32) + mixer_sum).astype(jnp.bfloat16)
    normed_mlp = rms_scale(middle, mlp_gain)
    local_units = gate_weight.shape[1]
    both = jnp.dot(
        join_rows(normed_mlp),
        mlp_full,
        preferred_element_type=jnp.float32,
    )
    hidden_units = (jax.nn.silu(both[:, :local_units]) * both[:, local_units:]).astype(jnp.bfloat16)
    mlp_sum = share_sum(
        jnp.dot(hidden_units, down_full, preferred_element_type=jnp.float32).astype(jnp.bfloat16)
    )
    return (middle.astype(jnp.float32) + mlp_sum).astype(jnp.bfloat16)


def solution(mesh):
    placed = (
        P(("rep", "fs", "tp"), None),
        P(),
        P("fs", "tp"),
        P("fs", "tp"),
        P("fs", "tp"),
        P("tp"),
        P("tp", "fs"),
        P(),
        P("fs", "tp"),
        P("fs", "tp"),
        P("tp", "fs"),
    )
    return jax.shard_map(
        shards, mesh=mesh, in_specs=placed, out_specs=P(("rep", "fs", "tp"), None), check_vma=False
    )
```

time: 296 us -> 238 us (0.80)
  other arithmetic: 22.6 us -> 0 us
  matrix products: 21.3 us -> 0 us
  waiting for transfers between devices: 10.1 us -> 0 us
    dot_general x2 -> x0, matrix products: 21.3 us -> none  [the longest x1 12.5 us: shards(): jnp.dot(join_rows(normed_mlp), mlp_full, preferred_element_type=jnp.float32)]
    ppermute x4 -> x0, waiting for transfers between devices: 10.1 us -> none  [swap(): return lax.ppermute(rows, 'tp', [(0, 1), (1, 0)])]
    concatenate x3 -> x0, other arithmetic: 6.8 us -> none  [the longest x1 2.58 us: shards(): mlp_shard = jnp.concatenate([gate_weight, up_weight], axis=1)]
    convert_element_type x3 -> x0, other arithmetic: 5.39 us -> none  [the longest x2 3.41 us: rms_scale(): return (scaled * gain).astype(jnp.bfloat16)]
    reduce_sum x2 -> x0, other arithmetic: 4.34 us -> none  [rms_scale(): jnp.mean(widened * widened, axis=-1, keepdims=True) + norm_eps]
  transfers between devices with their start and end apart: 4 -> 0, of which waited for: 3 -> 0; matrix products, arithmetic and copies ran while one was open for 3% -> 0% of each run, Pallas kernels for 0% -> 0%
where the time goes in v1:
time: 238 us
  Pallas kernels  235 us (99%)
  local copies, waits for them, and re-layouts  2.73 us (1%)
    pallas_call x1, Pallas kernels, layer(): pl.pallas_call(functools.partial(layer_kernel, depth, streams, shapes, he...  235 us

profile of v1, /device:TPU:0, one launch (start us, length us, event | category | flops | bytes accessed | tf_op | source)
XLA Modules:
  0.0 238.0 jit_solution(7089441978154421111)
XLA Ops:
  0.0 235.2 %shard_map.127 = bf16[384,2048]{1,0:T(8,128)(2,1)} custom-call(bf16[384,2048]{1,0:T(8,128)(2,1)} %refs_0_.1, f32[1,2048]{1,0:T(1,128)} %bitcast.3, bf16[256,512]{1,0:T(8,128)(2,1)} %refs_2_.1, bf16[256,512]{1,0:T(8,128)(2,1)} %refs_3_.1, bf16[256,1024]{1,0:T(8,128)(2,1)} %refs_4_.1, f32[1,1024]{1,0:T(1,128)} %bitcast.5, bf16[1024,256]{1,0:T(8,128)(2,1)} %refs_6_.1, ...), custom_call_target="tpu_custom_call" | custom-call | tf_op jit(solution)/shard_map/pallas_call | solution.py:507
  235.2 2.7 %copy.15 = bf16[384,2048]{1,0:T(8,128)(2,1)} copy(bf16[384,2048]{1,0:T(8,128)(2,1)} %shard_map.127) | data formatting | bytes 3145728

commit v2 on v1

--- a/solution.py
+++ b/solution.py
@@ -161,10 +161,121 @@
             self.each(back, sent)
 
 
-class Peer:
-    def __init__(self, send_sem, recv_sem):
+class Halves:
+    def __init__(self, depth, gate_up, down, far_send, far_recv, send_sem, recv_sem, sizes):
+        self.depth, self.gate_up, self.down = depth, gate_up, down
+        self.far_send, self.far_recv = far_send, far_recv
         self.send_sem, self.recv_sem = send_sem, recv_sem
-        self.core = lax.axis_index("tp")
+        self.in_rows, self.out_cols = sizes
+        self.x = lax.axis_index("rep")
+        fs = lax.axis_index("fs")
+        self.z = fs // 2
+        self.y = lax.rem(fs, 2)
+
+    def near(self, rank):
+        orders = []
+        for z in range(self.depth):
+            orders.append(sorted(range(self.depth), key=lambda other: (abs(other - z), other)))
+        code = sum(orders[z][rank] * self.depth**z for z in range(self.depth))
+        place = 0
+        for z in range(self.depth):
+            digit = code // self.depth**z % self.depth
+            place = place + digit * jnp.where(self.z == z, 1, 0)
+        return place
+
+    def block(self, s, origin):
+        return origin * 2 + (self.y if s % 2 == 0 else 1 - self.y)
+
+    def place(self, s, origin, side):
+        block = self.block(s, origin)
+        if s < 2:
+            half = self.in_rows // 2
+            start = pl.multiple_of(block * self.in_rows + side * half, 16)
+            return self.gate_up.at[pl.ds(start, half), :]
+        half = self.down.shape[0] // 2
+        return self.down.at[
+            pl.ds(pl.multiple_of(side * half, 16), half),
+            pl.ds(pl.multiple_of(block * self.out_cols, 128), self.out_cols),
+        ]
+
+    def cross(self, part, incoming=False):
+        mine = self.z * 2 + self.y
+        block = self.z * 2 + 1 - self.y if incoming else mine
+        if part < 4:
+            count = self.in_rows // 4
+            source = self.other_gate_up.at[pl.ds(part * count, count), :]
+            start = pl.multiple_of(block * self.in_rows + part * count, 16)
+            place = self.gate_up.at[pl.ds(start, count), :]
+        else:
+            source = self.other_down
+            place = self.down.at[
+                :, pl.ds(pl.multiple_of(block * self.out_cols, 128), self.out_cols)
+            ]
+        return pltpu.make_async_remote_copy(
+            src_ref=source,
+            dst_ref=place,
+            send_sem=self.far_send.at[part],
+            recv_sem=self.far_recv.at[part],
+            device_id={"fs": self.z * 2 + 1 - self.y},
+            device_id_type=MESH,
+        )
+
+    def copy(self, s, kind, origin, incoming=False):
+        x, y, z = self.x, self.y, self.z
+        side = 1 - x if incoming and kind == "x" else x
+        target = {
+            "up": {"fs": (z + 1) * 2 + y},
+            "down": {"fs": (z - 1) * 2 + y},
+            "x": {"rep": 1 - x},
+        }[kind]
+        place = self.place(s, origin, side)
+        sends = ("up", "down", "x").index(kind)
+        receives = (0, 0, 1)[sends]
+        return pltpu.make_async_remote_copy(
+            src_ref=place,
+            dst_ref=place,
+            send_sem=self.send_sem.at[s, sends, origin],
+            recv_sem=self.recv_sem.at[s, receives, origin],
+            device_id=target,
+            device_id_type=MESH,
+        )
+
+    each = Exchange.each
+    onward = Exchange.onward
+
+    def step(self, s, t):
+        def arrive(way, origin):
+            if way != "own":
+                self.copy(s, way, origin, incoming=True).wait_recv()
+            self.onward(s, way, origin, lambda c: c.start())
+            if way != "own":
+                self.copy(s, "x", origin).start()
+
+        self.each(t, arrive)
+
+    def joined(self, s):
+        for rank in range(1, self.depth):
+            self.copy(s, "x", self.near(rank), incoming=True).wait_recv()
+
+    def drain(self, s):
+        for back in range(self.depth):
+
+            def sent(way, origin):
+                self.onward(s, way, origin, lambda c: c.wait_send())
+                if way != "own":
+                    self.copy(s, "x", origin).wait_send()
+
+            self.each(back, sent)
+
+
+class Near:
+    def __init__(self, axis, send_sem, recv_sem):
+        self.send_sem, self.recv_sem = send_sem, recv_sem
+        if axis == "tp":
+            self.target = {"tp": 1 - lax.axis_index("tp")}
+        else:
+            fs = lax.axis_index("fs")
+            self.target = {"fs": fs // 2 * 2 + 1 - lax.rem(fs, 2)}
 
     def copy(self, index, source, place):
         return pltpu.make_async_remote_copy(
@@ -172,7 +283,7 @@
             dst_ref=place,
             send_sem=self.send_sem.at[index],
             recv_sem=self.recv_sem.at[index],
-            device_id={"tp": 1 - self.core},
+            device_id=self.target,
             device_id_type=MESH,
         )
 
@@ -185,8 +296,8 @@
     )
 
 
-def column_dot(left, right, out, first, last, width=256):
-    @pl.loop(first, last)
+def column_dot(left, right, out, width=256):
+    @pl.loop(0, out.shape[1] // width)
     def _(c):
         cols = pl.ds(pl.multiple_of(c * width, width), width)
         out[:, cols] = jnp.dot(
@@ -219,82 +330,141 @@
         key_decay[h] = jnp.exp(rate * (block - 1.0 - row))
 
 
-def retain_blocks(h, heads, first, last, tables, proj, memory, head_out):
-    cos_ref, sin_ref, inside, query_decay, key_decay, gain = tables
+def weigh_blocks(heads, tables, pairs, weights, decayed):
+    cos_ref, sin_ref, inside, _, key_decay = tables
+    block = inside.shape[-1]
+
+    @pl.loop(0, pairs.shape[0] // block)
+    def _(b):
+        rows = pl.ds(pl.multiple_of(b * block, block), block)
+        cosine, sine = cos_ref[rows, :], sin_ref[rows, :]
+        for h in range(heads):
+            q_cols = pl.ds(h * DK, DK)
+            k_cols = pl.ds((heads + h) * DK, DK)
+            q = rotated(pairs[rows, q_cols].astype(jnp.float32), cosine, sine)
+            q = q.astype(jnp.bfloat16)
+            k = rotated(pairs[rows, k_cols].astype(jnp.float32), cosine, sine) * DK ** (-0.5)
+            k = k.astype(jnp.bfloat16)
+            scores = lax.dot_general(
+                q, k, (((1,), (1,)), ((), ())), preferred_element_type=jnp.float32
+            )
+            pairs[rows, q_cols] = q
+            weights[rows, pl.ds(h * block, block)] = (scores * inside[h]).astype(jnp.bfloat16)
+            decayed[rows, q_cols] = (
+                k.astype(jnp.float32) * key_decay[h][:, 0:1]
+            ).astype(jnp.bfloat16)
+
+
+def retain_blocks(heads, first, last, tables, gain, held, memory, head_out):
+    pairs, weights, decayed, values = held
+    inside, query_decay = tables[2], tables[3]
     core = lax.axis_index("tp")
     block = inside.shape[-1]
     rates = decay_rates(range(2 * heads))
-    block_decay = jnp.where(
-        core == 0, math.exp(rates[h] * block), math.exp(rates[heads + h] * block)
-    )
     if first == 0:
         memory[...] = jnp.zeros_like(memory)
-    q_cols = pl.ds(h * DK, DK)
-    k_cols = pl.ds((heads + h) * DK, DK)
-    v_cols = pl.ds(2 * heads * DK + h * DV, DV)
 
     @pl.loop(first, last)
     def _(b):
         rows = pl.ds(pl.multiple_of(b * block, block), block)
-        cosine, sine = cos_ref[rows, :], sin_ref[rows, :]
-        q = rotated(proj[rows, q_cols].astype(jnp.float32), cosine, sine).astype(jnp.bfloat16)
-        k = rotated(proj[rows, k_cols].astype(jnp.float32), cosine, sine) * DK ** (-0.5)
-        k = k.astype(jnp.bfloat16)
-        v = proj[rows, v_cols]
-        scores = lax.dot_general(
-            q, k, (((1,), (1,)), ((), ())), preferred_element_type=jnp.float32
-        )
-        weights = (scores * inside[h]).astype(jnp.bfloat16)
-        state = memory[...]
-        kept = jnp.dot(weights, v, preferred_element_type=jnp.float32) + query_decay[h][
-            :, 0:1
-        ] * jnp.dot(q, state.astype(jnp.bfloat16), preferred_element_type=jnp.float32)
-        decayed = (k.astype(jnp.float32) * key_decay[h][:, 0:1]).astype(jnp.bfloat16)
-        memory[...] = state * block_decay + lax.dot_general(
-            decayed, v, (((0,), (0,)), ((), ())), preferred_element_type=jnp.float32
-        )
-        scale = lax.rsqrt(jnp.mean(kept * kept, axis=-1, keepdims=True) + norm_eps)
-        head_out[rows, pl.ds(h * DV, DV)] = (
-            kept * scale * gain[:, pl.ds(h * DV, DV)]
-        ).astype(jnp.bfloat16)
+        for h in range(heads):
+            block_decay = jnp.where(
+                core == 0, math.exp(rates[h] * block), math.exp(rates[heads + h] * block)
+            )
+            v_cols = pl.ds(h * DV, DV)
+            v = values[rows, v_cols]
+            state = memory[h]
+            kept = jnp.dot(
+                weights[rows, pl.ds(h * block, block)], v, preferred_element_type=jnp.float32
+            ) + query_decay[h][:, 0:1] * jnp.dot(
+                pairs[rows, pl.ds(h * DK, DK)],
+                state.astype(jnp.bfloat16),
+                preferred_element_type=jnp.float32,
+            )
+            memory[h] = state * block_decay + lax.dot_general(
+                decayed[rows, pl.ds(h * DK, DK)],
+                v,
+                (((0,), (0,)), ((), ())),
+                preferred_element_type=jnp.float32,
+            )
+            scale = lax.rsqrt(jnp.mean(kept * kept, axis=-1, keepdims=True) + norm_eps)
+            head_out[rows, v_cols] = (kept * scale * gain[:, v_cols]).astype(jnp.bfloat16)
 
 
 ROWS = 64
 WIDE = 512
+TILE = 128
+SHARED = 3
 
 
 def layer_kernel(depth, streams, shapes, heads, *refs):
     args, refs = refs[:13], refs[13:]
     resid, mix_gain, query, key, value, head_gain, out_w, mlp_gain, gate, up, down, cos, sin = args
     out, refs = refs[0], refs[1:]
-    fulls, refs = refs[:4], refs[4:]
-    mixer, out_full, mlp, down_full = fulls
-    held, refs = refs[:6], refs[6:]
-    x, gain_mix, gain_head, gain_mlp, cos_v, sin_v = held
-    normed, both, proj, memory, head_out, hidden, part, sent, got, middle, result, refs = (
-        *refs[:11],
-        refs[11:],
+    fulls, refs = refs[:3], refs[3:]
+    pair_full, value_full, out_full = fulls
+    gate_up, other_gate_up, down_full, other_down, refs = *refs[:4], refs[4:]
+    x, gain_mix, gain_head, gain_mlp, cos_v, sin_v, middle_gate, middle_up, refs = (
+        *refs[:8],
+        refs[8:],
+    )
+    normed, both, pairs, values, weights, decayed, memory, head_out, hidden, refs = (
+        *refs[:9],
+        refs[9:],
+    )
+    part, sent, got, far_part, far_sent, far_got, far_sum, far_in, middle, refs = (
+        *refs[:9],
+        refs[9:],
     )
     inside, query_decay, key_decay, refs = *refs[:3], refs[3:]
-    send_sem, recv_sem, load_sem, peer_send, peer_recv, out_sem = refs
-    ex = Exchange(depth, streams, shapes, (0, 1, 0, 1), fulls, send_sem, recv_sem)
-    peer = Peer(peer_send, peer_recv)
+    send_sem, recv_sem, half_send, half_recv, cross_send, cross_recv, refs = *refs[:6], refs[6:]
+    load_sem, peer_send, peer_recv, beside_send, beside_recv, out_sem = refs
+
+    ex = Exchange(depth, streams, shapes, (0, 0, 1), fulls, send_sem, recv_sem)
+    sizes = (gate.shape[0], down.shape[1])
+    hv = Halves(
+        depth, gate_up, down_full, cross_send, cross_recv, half_send, half_recv, sizes
+    )
+    hv.other_gate_up, hv.other_down = other_gate_up, other_down
+    peer = Near("tp", peer_send, peer_recv)
+    beside = Near("fs", beside_send, beside_recv)
     core = lax.axis_index("tp")
     fs = lax.axis_index("fs")
-    rows = x.shape[0]
-    qc, kc, vc = query.shape[1], key.shape[1], value.shape[1]
+    y = lax.rem(fs, 2)
+    rows, width = x.shape
+    qc, kc = query.shape[1], key.shape[1]
     units = gate.shape[1]
-
-    mixer_own = pl.ds(pl.multiple_of(fs * shapes[0][0], 16), shapes[0][0])
-    mlp_own = pl.ds(pl.multiple_of(fs * shapes[2][0], 16), shapes[2][0])
-    pairs = [
-        (query, mixer.at[mixer_own, pl.ds(0, qc)]),
-        (key, mixer.at[mixer_own, pl.ds(qc, kc)]),
-        (value, mixer.at[mixer_own, pl.ds(qc + kc, vc)]),
-        (out_w, ex.slot(1, fs, 0, shapes[1][0])),
+    whole = units // 2 // TILE
+    aligned = whole * TILE
+    step = aligned + TILE
+    blocks = width // sizes[1]
+
+    own_rows = ex.slot(0, fs, 0, shapes[0][0])
+    first_row = pl.multiple_of(fs * shapes[0][0], 16)
+    own_pair = pl.ds(first_row, shapes[0][0])
+    own_cols = pl.ds(pl.multiple_of(fs * sizes[1], 128), sizes[1])
+
+    def down_pieces(side, place):
+        rest = units // 2 - aligned
+        return [
+            (down.at[pl.ds(pl.multiple_of(side * step, 16), aligned), :], place(0, aligned)),
+            (
+                down.at[pl.ds(pl.multiple_of(aligned + side * rest, 16), rest), :],
+                place(aligned, rest),
+            ),
+        ]
+
+    moves = [
+        (query, pair_full.at[own_pair, pl.ds(0, qc)]),
+        (key, pair_full.at[own_pair, pl.ds(qc, kc)]),
+        (value, ex.slot(1, fs, 0, shapes[1][0])),
         (resid, x),
         (mix_gain, gain_mix),
-        (down, ex.slot(3, fs, 0, shapes[3][0])),
+        (out_w, ex.slot(2, fs, 0, shapes[2][0])),
+        (gate.at[:, pl.ds(aligned, TILE)], middle_gate),
+        (up.at[:, pl.ds(aligned, TILE)], middle_up),
+        *down_pieces(y, lambda start, count: down_full.at[pl.ds(start, count), own_cols]),
+        *down_pieces(1 - y, lambda start, count: other_down.at[pl.ds(start, count), :]),
         (cos, cos_v),
         (sin, sin_v),
         (head_gain, gain_head),
@@ -302,35 +472,39 @@
     ]
     loads = [
         pltpu.make_async_copy(source, place, load_sem.at[i])
-        for i, (source, place) in enumerate(pairs)
+        for i, (source, place) in enumerate(moves)
     ]
-    for load in loads[:6]:
+    for load in loads[:8]:
         load.start()
-
-    @pl.loop(0, units // 128)
-    def _(j):
-        cols = pl.ds(pl.multiple_of(j * 128, 128), 128)
-        for i, source in enumerate((gate, up)):
-            place = pl.ds(pl.multiple_of(j * 256, 128) + i * 128, 128)
-            pltpu.make_async_copy(
-                source.at[:, cols], mlp.at[mlp_own, place], load_sem.at[len(pairs)]
-            ).start()
-
-    for load in loads[6:]:
+    own_gate_up = gate_up.at[own_pair, :]
+    gathers = []
+    for side, target, index in ((y, own_gate_up, 0), (1 - y, other_gate_up, 1)):
+        sem = load_sem.at[len(moves) + index]
+
+        @pl.loop(0, whole)
+        def _(j):
+            cols = pl.ds(pl.multiple_of(side * step + j * TILE, TILE), TILE)
+            for i, source in enumerate((gate, up)):
+                place = pl.ds(pl.multiple_of(j * 2 * TILE, TILE) + i * TILE, TILE)
+                pltpu.make_async_copy(source.at[:, cols], target.at[:, place], sem).start()
+
+        bulk = target.at[:, pl.ds(0, 2 * aligned)]
+        gathers.append(pltpu.make_async_copy(bulk, bulk, sem))
+    for load in loads[8:]:
         load.start()
-    mlp_slot = ex.slot(2, fs, 0, shapes[2][0])
-    mlp_load = pltpu.make_async_copy(mlp_slot, mlp_slot, load_sem.at[len(pairs)])
 
     ex.barrier()
+
+    def chip_rows(side, of):
+        return pl.ds(pl.multiple_of((side * 2 + of) * rows, 16), rows)
 
     own = pl.ds(pl.multiple_of(core * rows, 16), rows)
     other = pl.ds(pl.multiple_of((1 - core) * rows, 16), rows)
     join_mix = peer.copy(0, normed.at[own, :], normed.at[own, :])
-    join_mlp = peer.copy(1, both.at[own, :], both.at[own, :])
 
     def norm_mix():
+        loads[3].wait()
         loads[4].wait()
-        loads[5].wait()
 
         @pl.loop(0, rows // ROWS)
         def _(r):
@@ -339,137 +513,281 @@
             normed[there, :] = scaled_rows(x[here, :].astype(jnp.float32), gain_mix[...])
 
         join_mix.start()
+        loads[6].wait()
+        loads[7].wait()
+        half = TILE // 2
+        low_gate = middle_gate[...].astype(jnp.float32)
+        low_up = middle_up[...].astype(jnp.float32)
+        first = jnp.concatenate([low_gate[:, :half], low_up[:, :half]], axis=1)
+        second = jnp.concatenate([low_gate[:, half:], low_up[:, half:]], axis=1)
+        end = pl.ds(2 * aligned, TILE)
+        mine = jnp.where(y == 0, first, second)
+        theirs = jnp.where(y == 0, second, first)
+        gate_up[own_pair, end] = mine.astype(jnp.bfloat16)
+        other_gate_up[:, end] = theirs.astype(jnp.bfloat16)
         make_tables(heads, inside, query_decay, key_decay)
-        for load in loads[7:]:
+        for load in loads[12:]:
             load.wait()
+        for load in gathers:
+            load.wait()
+
+    def cross(parts):
+        for part_index in parts:
+            if part_index == 4:
+                for load in loads[8:12]:
+                    load.wait()
+            hv.cross(part_index).start()
+
+    tables = (cos_v, sin_v, inside, query_decay, key_decay)
+    held = (pairs, weights, decayed, values)
+
+    def project_pairs():
+        join_mix.wait()
+        column_dot(normed, pair_full, pairs)
+        weigh_blocks(heads, tables, pairs, weights, decayed)
+
+    def project_values():
+        column_dot(normed, value_full, values)
+
+    def retain_some(first, last):
+        retain_blocks(heads, first, last, tables, gain_head, held, memory, head_out)
+
+    chunks = width // WIDE
 
     def share(index, c):
         cols = pl.ds(c * WIDE, WIDE)
         return peer.copy(index + c, sent.at[:, cols], got.at[:, cols])
 
-    chunks = part.shape[1] // WIDE
-
-    def product(left, right, index):
-        for c in range(chunks):
-
-            @pl.loop(0, WIDE // 256)
-            def _(i):
-                cols = pl.ds(pl.multiple_of(c * WIDE + i * 256, 256), 256)
-                sent[:, cols] = jnp.dot(
-                    left[other, :], right[:, cols], preferred_element_type=jnp.float32
-                ).astype(jnp.bfloat16)
-
-            share(index, c).start()
-        for c in range(chunks):
-
-            @pl.loop(0, WIDE // 256)
-            def _(i):
-                cols = pl.ds(pl.multiple_of(c * WIDE + i * 256, 256), 256)
-                part[:, cols] = jnp.dot(
-                    left[own, :], right[:, cols], preferred_element_type=jnp.float32
-                ).astype(jnp.bfloat16)
+    def product(left, theirs, mine, right, index):
+        for rows_of, place in ((theirs, sent), (mine, part)):
+            for c in range(chunks):
+
+                @pl.loop(0, WIDE // 256)
+                def _(i):
+                    cols = pl.ds(pl.multiple_of(c * WIDE + i * 256, 256), 256)
+                    place[:, cols] = jnp.dot(
+                        left[rows_of, :], right[:, cols], preferred_element_type=jnp.float32
+                    ).astype(jnp.bfloat16)
+
+                if place is sent:
+                    share(index, c).start()
+
+    def shared_rows(side, of, i):
+        count = rows // SHARED
+        start = pl.multiple_of((side * 2 + of) * rows + i * count, 16)
+        return both.at[pl.ds(start, count), :]
+
+    def join_own(i, of):
+        place = shared_rows(y, of, i)
+        return peer.copy(1 + i, place, place)
+
+    def join_far(i, of):
+        place = shared_rows(1 - y, of, i)
+        return peer.copy(1 + SHARED + i, place, place)
+
+    def join_beside(i, side):
+        place = shared_rows(side, core, i)
+        return beside.copy(i, place, place)
+
+    base = 1 + 2 * SHARED
 
     def norm_mlp():
         for c in range(chunks):
-            share(2, c).wait()
-
-        @pl.loop(0, rows // ROWS)
-        def _(r):
-            here = pl.ds(pl.multiple_of(r * ROWS, ROWS), ROWS)
-            there = pl.ds(pl.multiple_of(core * rows + r * ROWS, ROWS), ROWS)
-            total = part[here, :].astype(jnp.float32) + got[here, :].astype(jnp.float32)
-            mid = (x[here, :].astype(jnp.float32) + total).astype(jnp.bfloat16)
-            middle[here, :] = mid
-            both[there, :] = scaled_rows(mid.astype(jnp.float32), gain_mlp[...])
-
-        join_mlp.start()
-
-    def expand():
-        @pl.loop(0, units // 128)
+            share(base, c).wait()
+        count = rows // SHARED
+        for i in range(SHARED):
+
+            @pl.loop(0, count // ROWS)
+            def _(r):
+                at = i * count + r * ROWS
+                here = pl.ds(pl.multiple_of(at, ROWS), ROWS)
+                there = pl.ds(pl.multiple_of((y * 2 + core) * rows + at, ROWS), ROWS)
+                total = part[here, :].astype(jnp.float32) + got[here, :].astype(jnp.float32)
+                mid = (x[here, :].astype(jnp.float32) + total).astype(jnp.bfloat16)
+                middle[here, :] = mid
+                both[there, :] = scaled_rows(mid.astype(jnp.float32), gain_mlp[...])
+
+            join_beside(i, y).start()
+            join_own(i, core).start()
+
+    def pass_on(i):
+        join_beside(i, 1 - y).wait_recv()
+        join_far(i, core).start()
+
+    def expand(side):
+        tokens = pl.ds(pl.multiple_of(side * 2 * rows, 16), 2 * rows)
+
+        @pl.loop(0, whole)
         def _(j):
-            cols = pl.ds(pl.multiple_of(j * 256, 256), 256)
-            pair = jnp.dot(both[...], mlp[:, cols], preferred_element_type=jnp.float32)
-            place = pl.ds(pl.multiple_of(j * 128, 128), 128)
-            hidden[:, place] = (jax.nn.silu(pair[:, :128]) * pair[:, 128:]).astype(jnp.bfloat16)
+            cols = pl.ds(pl.multiple_of(j * 2 * TILE, 2 * TILE), 2 * TILE)
+            two = jnp.dot(both[tokens, :], gate_up[:, cols], preferred_element_type=jnp.float32)
+            place = pl.ds(pl.multiple_of(j * TILE, TILE), TILE)
+            hidden[tokens, place] = (jax.nn.silu(two[:, :TILE]) * two[:, TILE:]).astype(
+                jnp.bfloat16
+            )
+
+        two = jnp.dot(
+            both[tokens, :],
+            gate_up[:, pl.ds(2 * aligned, TILE)],
+            preferred_element_type=jnp.float32,
+        )
+        half = TILE // 2
+        hidden[tokens, pl.ds(aligned, half)] = (
+            jax.nn.silu(two[:, :half]) * two[:, half:]
+        ).astype(jnp.bfloat16)
+
+    def expand_far():
+        for s in (0, 1):
+            hv.joined(s)
+        for i in range(SHARED):
+            join_far(i, 1 - core).wait_recv()
+        expand(1 - y)
+
+    def block_cols(block):
+        return pl.ds(pl.multiple_of(block * sizes[1], 128), sizes[1])
+
+    over = base + chunks
+
+    def swap_far(block):
+        cols = block_cols(block)
+        return peer.copy(over + block, far_sent.at[:, cols], far_got.at[:, cols])
+
+    def give(block):
+        cols = block_cols(block)
+        return beside.copy(SHARED + block, far_sum.at[:, cols], far_in.at[:, cols])
+
+    def reduce_far(block):
+        cols = block_cols(block)
+        far_sent[:, cols] = jnp.dot(
+            hidden[chip_rows(1 - y, 1 - core), :],
+            down_full[:, cols],
+            preferred_element_type=jnp.float32,
+        ).astype(jnp.bfloat16)
+        swap_far(block).start()
+        far_part[:, cols] = jnp.dot(
+            hidden[chip_rows(1 - y, core), :],
+            down_full[:, cols],
+            preferred_element_type=jnp.float32,
+        ).astype(jnp.bfloat16)
+
+    def give_far(block):
+        cols = block_cols(block)
+        swap_far(block).wait_recv()
+        total = far_part[:, cols].astype(jnp.float32) + far_got[:, cols].astype(jnp.float32)
+        far_sum[:, cols] = total.astype(jnp.bfloat16)
+        give(block).start()
+
+    def reduce_rank(rank):
+        origin = hv.near(rank)
+        for s in (2, 3):
+            if rank == 0 and s == 3:
+                pass
+            if rank > 0:
+                hv.copy(s, "x", origin, incoming=True).wait_recv()
+            reduce_far(hv.block(s, origin))
+        for s in (2, 3):
+            give_far(hv.block(s, origin))
+
+    last = over + blocks
+
+    def own_part():
+        for i in range(SHARED):
+            join_own(i, 1 - core).wait_recv()
+        expand(y)
+        product(hidden, chip_rows(y, 1 - core), chip_rows(y, core), down_full, last)
 
     def finish():
         writes = []
         for c in range(chunks):
-            cols = pl.ds(c * WIDE, WIDE)
-            share(2 + chunks, c).wait()
-            total = part[:, cols].astype(jnp.float32) + got2(cols)
-            result[:, cols] = (middle[:, cols].astype(jnp.float32) + total).astype(jnp.bfloat16)
-            write = pltpu.make_async_copy(result.at[:, cols], out.at[:, cols], out_sem.at[c])
-            write.start()
-            writes.append(write)
+            share(last, c).wait()
+        for rank in range(depth):
+            origin = hv.near(rank)
+            for s in (3, 2):
+                block = hv.block(s, origin)
+                cols = block_cols(block)
+                give(block).wait_recv()
+                total = part[:, cols].astype(jnp.float32) + got[:, cols].astype(jnp.float32)
+                total = total + far_in[:, cols].astype(jnp.float32)
+                middle[:, cols] = (middle[:, cols].astype(jnp.float32) + total).astype(
+                    jnp.bfloat16
+                )
+                write = pltpu.make_async_copy(
+                    middle.at[:, cols], out.at[:, cols], out_sem.at[block]
+                )
+                write.start()
+                writes.append(write)
         for write in writes:
             write.wait()
 
-    def got2(cols):
-        return got[:, cols].astype(jnp.float32)
-
-    blocks = proj.shape[0] // inside.shape[-1]
-    tables = (cos_v, sin_v, inside, query_decay, key_decay, gain_head)
-    columns = proj.shape[1] // 256
-    plan = {0: [norm_mix]}
-    span = 2 * (depth + 2) - 6
-    half = blocks // 2
-    first = 2 * (depth + 1) + 1
-
-    def project(low, high):
-        if low == 0:
-            join_mix.wait()
-        column_dot(normed, mixer, proj, low, high)
-
-    plan[first] = [lambda: project(0, columns // 2)]
-    plan[first + 1] = [lambda: project(columns // 2, columns)]
-    at = first + 2
-    for h in range(heads):
-        for low, high in ((0, half), (half, blocks)):
-            plan.setdefault(at, []).append(
-                functools.partial(
-                    retain_blocks, h, heads, low, high, tables, proj, memory, head_out
-                )
-            )
-            at += 1
-    plan.setdefault(first + 6, []).append(lambda: product(head_out, out_full, 2))
-    plan.setdefault(first + 7, []).append(norm_mlp)
-
-    def mlp_in():
-        join_mlp.wait()
-        expand()
-
-    plan.setdefault(first + 12, []).append(mlp_in)
-    plan.setdefault(first + 18, []).append(lambda: product(hidden, down_full, 2 + chunks))
-    plan[first + 18].append(finish)
-    count = len(streams)
-    begin = {0: loads[:3], 2: loads[3:4], 4: [mlp_load], 6: loads[6:7]}
-    for tick in range(first + 19):
-        for s in range(count):
-            t, odd = divmod(tick - 6 * (s // 2), 2)
+    plan = {}
+
+    def at(tick, *jobs):
+        plan.setdefault(tick, []).extend(jobs)
+
+    stages = len(streams) // 2
+    turn = 2 * (depth - 1)
+    at(0, norm_mix)
+    for i in range(4):
+        at(2 + i, functools.partial(cross, (i,)))
+    at(8, functools.partial(cross, (4,)))
+    at(turn + 4, project_pairs)
+    at(turn + 5, project_values)
+    length = pairs.shape[0] // inside.shape[-1]
+    at(turn + 6, functools.partial(retain_some, 0, length // 2))
+    at(turn + 7, functools.partial(retain_some, length // 2, length))
+    at(
+        2 * turn + 5,
+        lambda: product(head_out, other, own, out_full, base),
+        norm_mlp,
+    )
+    mlp_at = stages * turn
+    at(2 * turn + 7, functools.partial(pass_on, 0))
+    at(2 * turn + 8, functools.partial(pass_on, 1))
+    at(mlp_at + turn + 3, functools.partial(pass_on, 2), expand_far)
+    at(mlp_at + turn + 3, functools.partial(reduce_rank, 0))
+    at(mlp_at + turn + 4, functools.partial(reduce_rank, 1))
+    at(mlp_at + turn + 5, functools.partial(reduce_rank, 2))
+    at(mlp_at + turn + 7, functools.partial(reduce_rank, 3), own_part, finish)
+    begin = {0: loads[:2], 1: loads[2:3], 2: loads[5:6]}
+    for tick in range(mlp_at + 2 * turn + 2):
+        for s in range(len(streams)):
+            t, odd = divmod(tick - turn * (s // 2), 2)
             if odd == s % 2 and 0 <= t <= depth + 1:
                 if t == 0:
                     for load in begin.get(s, ()):
                         load.wait()
                 ex.step(s, t)
+        for s in range(4):
+            t, odd = divmod(tick - mlp_at - turn * (s // 2), 2)
+            if odd == s % 2 and 0 <= t < depth:
+                if t == 0 and s % 2 == 1:
+                    for part_index in range(4) if s == 1 else (4,):
+                        hv.cross(part_index, incoming=True).wait_recv()
+                hv.step(s, t)
         for job in plan.get(tick, ()):
             job()
-    for s in range(count):
+    for s in range(len(streams)):
         ex.drain(s)
-
-
-def cut(total):
-    whole = total // (UNITS * 16)
-    first = (whole + 1) // 2 * UNITS * 16
-    return first, total - first
+    for s in range(4):
+        hv.drain(s)
+    for part_index in range(5):
+        hv.cross(part_index).wait_send()
+    for i in range(SHARED):
+        join_own(i, core).wait_send()
+        join_far(i, core).wait_send()
+        join_beside(i, y).wait_send()
+    for block in range(blocks):
+        swap_far(block).wait_send()
+        give(block).wait_send()
 
 
 def plan_streams(shapes):
     streams = []
-    for w, (rows, _) in enumerate(shapes):
-        first, second = cut(rows)
-        streams.append(Stream(w, 0, first, 6, 5))
-        streams.append(Stream(w, first, second, 7, 4))
+    for w, (rows, _) in enumerate(shapes[:2]):
+        streams.append(Stream(w, 0, rows, 6 + w, 4))
+    half = shapes[2][0] // 2
+    streams.append(Stream(2, 0, half, 6, 4))
+    streams.append(Stream(2, half, half, 7, 4))
     return streams
 
 
@@ -480,22 +798,24 @@
     return np.cos(angle).astype(np.float32), np.sin(angle).astype(np.float32)
 
 
-def fits(shapes, rows, heads):
-    whole = all(r % (UNITS * 16) == 0 and r >= 2 * UNITS * 16 and c % 128 == 0 for r, c in shapes)
-    sizes = lax.axis_size("rep") == 2 and lax.axis_size("fs") == 8 and lax.axis_size("tp") == 2
-    return whole and sizes and rows % BLOCK == 0 and heads == 2
+def fits(shapes, rows, width, heads, units):
+    whole = all(r % (2 * UNITS * 16) == 0 and c % 128 == 0 for r, c in shapes)
+    axes = lax.axis_size("rep") == 2 and lax.axis_size("fs") == 8 and lax.axis_size("tp") == 2
+    cut = units % (2 * TILE) == TILE and width % WIDE == 0 and width == 8 * shapes[2][1]
+    return whole and axes and cut and rows % (SHARED * ROWS) == 0 and heads == 2
 
 
 def layer(args, shapes, heads):
-    resid, query, key, value, gate = args[0], args[2], args[3], args[4], args[8]
+    resid, gate, down = args[0], args[8], args[10]
     size = lax.axis_size("fs")
     depth = size // 2
     rows, width = resid.shape
     length_total = 2 * rows
+    units = gate.shape[1]
     streams = plan_streams(shapes)
     count = len(streams)
     fulls = []
-    for (r, c), axis in zip(shapes, (0, 1, 0, 1)):
+    for (r, c), axis in zip(shapes, (0, 0, 1)):
         fulls.append((r * size, c) if axis == 0 else (r, c * size))
     cosine, sine = rotation_tables(length_total, DK // 2)
     far = pl.BlockSpec(memory_space=pl.ANY)
@@ -503,6 +823,7 @@
     vm = pltpu.VMEM
     dma = pltpu.SemaphoreType.DMA
     chunks = width // WIDE
+    peers = 1 + 2 * SHARED + 2 * chunks + size
     args = [a[None, :] if a.ndim == 1 else a for a in args]
     return pl.pallas_call(
         functools.partial(layer_kernel, depth, streams, shapes, heads),
@@ -511,32 +832,43 @@
         out_specs=far,
         scratch_shapes=[vm(s, bf) for s in fulls]
         + [
+            vm((gate.shape[0] * size, units), bf),
+            vm((gate.shape[0], units), bf),
+            vm((units // 2, width), bf),
+            vm((units // 2, down.shape[1]), bf),
             vm((rows, width), bf),
             vm(args[1].shape, f32),
             vm(args[5].shape, f32),
             vm(args[7].shape, f32),
             vm(cosine.shape, f32),
             vm(sine.shape, f32),
+            vm((gate.shape[0], TILE), bf),
+            vm((gate.shape[0], TILE), bf),
             vm((length_total, width), bf),
-            vm((length_total, width), bf),
+            vm((2 * length_total, width), bf),
             vm((length_total, shapes[0][1]), bf),
-            vm((DK, DV), f32),
+            vm((length_total, shapes[1][1]), bf),
+            vm((length_total, heads * BLOCK), bf),
+            vm((length_total, heads * DK), bf),
+            vm((heads, DK, DV), f32),
             vm((length_total, heads * DV), bf),
-            vm((length_total, gate.shape[1]), bf),
-            vm((rows, width), bf),
-            vm((rows, width), bf),
-            vm((rows, width), bf),
-            vm((rows, width), bf),
-            vm((rows, width), bf),
-            vm((heads, BLOCK, BLOCK), f32),
-            vm((heads, BLOCK, BLOCK), f32),
-            vm((heads, BLOCK, BLOCK), f32),
+            vm((2 * length_total, units // 2), bf),
+        ]
+        + [vm((rows, width), bf)] * 9
+        + [vm((heads, BLOCK, BLOCK), f32)] * 3
+        + [
             dma((count, 5, depth)),
             dma((count, 4, depth)),
-            dma((12,)),
-            dma((2 + 2 * chunks,)),
-            dma((2 + 2 * chunks,)),
-            dma((chunks,)),
+            dma((4, 3, depth)),
+            dma((4, 2, depth)),
+            dma((5,)),
+            dma((5,)),
+            dma((18,)),
+            dma((peers,)),
+            dma((peers,)),
+            dma((SHARED + size,)),
+            dma((SHARED + size,)),
+            dma((size,)),
         ],
         compiler_params=pltpu.CompilerParams(
             collective_id=0, has_side_effects=True, vmem_limit_bytes=67043328
@@ -677,12 +1009,11 @@
     key_cols = query_weight.shape[1]
     heads_here = key_cols // DK
     shapes = [
-        (query_weight.shape[0], query_weight.shape[1] + key_weight.shape[1] + value_weight.shape[1]),
+        (query_weight.shape[0], query_weight.shape[1] + key_weight.shape[1]),
+        value_weight.shape,
         out_weight.shape,
-        (gate_weight.shape[0], gate_weight.shape[1] + up_weight.shape[1]),
-        down_weight.shape,
     ]
-    if fits(shapes, token_rows, heads_here):
+    if fits(shapes, token_rows, resid.shape[1], heads_here, gate_weight.shape[1]):
         args = [
             resid, mix_gain, query_weight, key_weight, value_weight, head_gain,
             out_weight, mlp_gain, gate_weight, up_weight, down_weight,

time: 238 us -> 223 us (0.937)
  Pallas kernels: 235 us -> 220 us
    pallas_call x1, Pallas kernels: 235 us -> 220 us  [layer(): pl.pallas_call(functools.partial(layer_kernel, depth, streams, shapes, he...]
where the time goes in v2:
time: 223 us
  Pallas kernels  220 us (99%)
  local copies, waits for them, and re-layouts  2.73 us (1%)
    pallas_call x1, Pallas kernels, layer(): pl.pallas_call(functools.partial(layer_kernel, depth, streams, shapes, he...  220 us

profile of v2, /device:TPU:0, one launch (start us, length us, event | category | flops | bytes accessed | tf_op | source)
XLA Modules:
  0.0 222.7 jit_solution(5914727834978972852)
XLA Ops:
  0.0 220.0 %shard_map.127 = bf16[384,2048]{1,0:T(8,128)(2,1)} custom-call(bf16[384,2048]{1,0:T(8,128)(2,1)} %refs_0_.1, f32[1,2048]{1,0:T(1,128)} %bitcast.3, bf16[256,512]{1,0:T(8,128)(2,1)} %refs_2_.1, bf16[256,512]{1,0:T(8,128)(2,1)} %refs_3_.1, bf16[256,1024]{1,0:T(8,128)(2,1)} %refs_4_.1, f32[1,1024]{1,0:T(1,128)} %bitcast.5, bf16[1024,256]{1,0:T(8,128)(2,1)} %refs_6_.1, ...), custom_call_target="tpu_custom_call" | custom-call | tf_op jit(solution)/shard_map/pallas_call | solution.py:828
  220.0 2.7 %copy.15 = bf16[384,2048]{1,0:T(8,128)(2,1)} copy(bf16[384,2048]{1,0:T(8,128)(2,1)} %shard_map.127) | data formatting | bytes 3145728

commit v3 on v0

v3 whole, which is shorter than its diff:
```python
import functools
import math

import jax
import jax.numpy as jnp
import numpy as np
from jax import lax
from jax.experimental import pallas as pl
from jax.experimental.pallas import tpu as pltpu
from jax.sharding import PartitionSpec as P

MESH = pl.DeviceIdType.MESH
ROWS = 64
TILE = 128


class Weight:
    def __init__(self, full, other, axis):
        self.full, self.other, self.axis = full, other, axis
        self.rows, self.cols = other.shape


class Gather:
    def __init__(self, depth, weights, along, cross_sems, sems):
        self.depth, self.weights, self.along = depth, weights, along
        self.cross_send, self.cross_recv = cross_sems
        self.send_sem, self.recv_sem = sems
        self.x = lax.axis_index("rep")
        fs = lax.axis_index("fs")
        self.z = fs // 2
        self.y = lax.rem(fs, 2)

    def barrier(self):
        sem = pltpu.get_barrier_semaphore()
        z, y, x = self.z, self.y, self.x
        core = lax.axis_index("tp")
        pl.semaphore_signal(sem, inc=1, device_id={"tp": 1 - core}, device_id_type=MESH)
        pl.semaphore_signal(sem, inc=1, device_id={"rep": 1 - x}, device_id_type=MESH)
        pl.semaphore_signal(sem, inc=1, device_id={"fs": z * 2 + 1 - y}, device_id_type=MESH)

        @pl.when(z > 0)
        def _():
            pl.semaphore_signal(sem, inc=1, device_id={"fs": (z - 1) * 2 + y}, device_id_type=MESH)

        @pl.when(z < self.depth - 1)
        def _():
            pl.semaphore_signal(sem, inc=1, device_id={"fs": (z + 1) * 2 + y}, device_id_type=MESH)

        low = jnp.minimum(z, 1)
        high = jnp.minimum(self.depth - 1 - z, 1)
        pl.semaphore_wait(sem, 3 + low + high)

    def near(self, rank):
        place = 0
        for z in range(self.depth):
            order = sorted(range(self.depth), key=lambda other: (abs(other - z), other))
            place = place + order[rank] * jnp.where(self.z == z, 1, 0)
        return place

    def block(self, far, origin):
        return origin * 2 + (1 - self.y if far else self.y)

    def place(self, w, block, start, count):
        weight = self.weights[w]
        if weight.axis == 0:
            first = pl.multiple_of(block * weight.rows + start, 16)
            return weight.full.at[pl.ds(first, count), :]
        cols = pl.ds(pl.multiple_of(block * weight.cols, 128), weight.cols)
        return weight.full.at[pl.ds(pl.multiple_of(start, 16), count), cols]

    def cross(self, s, incoming=False):
        w = s // 2
        count = self.along[w]
        start = pl.multiple_of((self.weights[w].rows - count) * self.x, 16)
        block = self.z * 2 + (1 - self.y if incoming else self.y)
        return pltpu.make_async_remote_copy(
            src_ref=self.weights[w].other.at[pl.ds(start, count), :],
            dst_ref=self.place(w, block, start, count),
            send_sem=self.cross_send.at[w],
            recv_sem=self.cross_recv.at[w],
            device_id={"fs": self.z * 2 + 1 - self.y},
            device_id_type=MESH,
        )

    def copy(self, s, kind, origin, incoming=False):
        w, far = s // 2, s % 2
        x, y, z = self.x, self.y, self.z
        rows, along = self.weights[w].rows, self.along[w]
        if kind == "x":
            count = rows - along
            start = along * (1 - x if incoming else x)
        else:
            count = along
            start = (rows - along) * x
        target = {
            "up": {"fs": (z + 1) * 2 + y},
            "down": {"fs": (z - 1) * 2 + y},
            "x": {"rep": 1 - x},
        }[kind]
        place = self.place(w, self.block(far, origin), start, count)
        sends = ("up", "down", "x").index(kind)
        receives = (0, 0, 1)[sends]
        return pltpu.make_async_remote_copy(
            src_ref=place,
            dst_ref=place,
            send_sem=self.send_sem.at[s, sends, origin],
            recv_sem=self.recv_sem.at[s, receives, origin],
            device_id=target,
            device_id_type=MESH,
        )

    def each(self, t, body):
        if t == 0:
            body("own", self.z)
            return

        @pl.when(self.z - t >= 0)
        def _():
            body("up", self.z - t)

        @pl.when(self.z + t < self.depth)
        def _():
            body("down", self.z + t)

    def onward(self, s, way, origin, act):
        if way in ("own", "up"):

            @pl.when(self.z < self.depth - 1)
            def _():
                act(self.copy(s, "up", origin))

        if way in ("own", "down"):

            @pl.when(self.z > 0)
            def _():
                act(self.copy(s, "down", origin))

    def arrive(self, s, t):
        def body(way, origin):
            if way != "own":
                self.copy(s, way, origin, incoming=True).wait_recv()
            elif s % 2:
                self.cross(s, incoming=True).wait_recv()
            self.onward(s, way, origin, lambda c: c.start())
            if way != "own" or s % 2:
                self.copy(s, "x", origin).start()

        self.each(t, body)

    def joined(self, s, rank):
        if rank > 0 or s % 2:
            self.copy(s, "x", self.near(rank), incoming=True).wait_recv()

    def drain(self, s):
        for back in range(self.depth):

            def sent(way, origin):
                self.onward(s, way, origin, lambda c: c.wait_send())
                if way != "own" or s % 2:
                    self.copy(s, "x", origin).wait_send()

            self.each(back, sent)
        if s % 2:
            self.cross(s).wait_send()


class Near:
    def __init__(self, axis, send_sem, recv_sem):
        self.send_sem, self.recv_sem = send_sem, recv_sem
        if axis == "tp":
            self.target = {"tp": 1 - lax.axis_index("tp")}
        else:
            fs = lax.axis_index("fs")
            self.target = {"fs": fs // 2 * 2 + 1 - lax.rem(fs, 2)}

    def copy(self, layer, index, source, place):
        return pltpu.make_async_remote_copy(
            src_ref=source,
            dst_ref=place,
            send_sem=self.send_sem.at[layer, index],
            recv_sem=self.recv_sem.at[layer, index],
            device_id=self.target,
            device_id_type=MESH,
        )


def rotated(v, cosine, sine):
    half = v.shape[-1] // 2
    first, second = v[:, :half], v[:, half:]
    return jnp.concatenate(
        [first * cosine - second * sine, second * cosine + first * sine], axis=-1
    )


def scaled_rows(values, gain):
    scale = lax.rsqrt(jnp.mean(values * values, axis=-1, keepdims=True) + norm_eps)
    return (values * scale * gain).astype(jnp.bfloat16)


def head_rate(scale, power=False):
    core = lax.axis_index("tp")
    y = lax.rem(lax.axis_index("fs"), 2)
    rates = [scale * math.log1p(-(2.0 ** (-5.0 - 2.0 * i))) for i in range(4)]
    if power:
        rates = [math.exp(r) for r in rates]
    return jnp.where(
        core == 0,
        jnp.where(y == 0, rates[0], rates[1]),
        jnp.where(y == 0, rates[2], rates[3]),
    )


def make_tables(inside, query_decay, key_decay):
    block = inside.shape[-1]
    row = lax.broadcasted_iota(jnp.int32, (block, block), 0).astype(jnp.float32)
    col = lax.broadcasted_iota(jnp.int32, (block, block), 1).astype(jnp.float32)
    distance = row - col
    rate = head_rate(1.0)
    inside[...] = jnp.where(distance >= 0, jnp.exp(rate * jnp.maximum(distance, 0.0)), 0.0)
    query_decay[...] = jnp.exp(rate * (row + 1.0))
    key_decay[...] = jnp.exp(rate * (block - 1.0 - row))


def weigh_blocks(start, length, tables, pairs, weights, decayed):
    cos_ref, sin_ref, inside, _, key_decay = tables
    block = inside.shape[-1]

    @pl.loop(0, length // block)
    def _(b):
        here = pl.ds(pl.multiple_of(b * block, block), block)
        rows = pl.ds(pl.multiple_of(start + b * block, block), block)
        cosine, sine = cos_ref[here, :], sin_ref[here, :]
        q = rotated(pairs[rows, pl.ds(0, DK)].astype(jnp.float32), cosine, sine)
        q = q.astype(jnp.bfloat16)
        k = rotated(pairs[rows, pl.ds(DK, DK)].astype(jnp.float32), cosine, sine) * DK ** (-0.5)
        k = k.astype(jnp.bfloat16)
        scores = lax.dot_general(
            q, k, (((1,), (1,)), ((), ())), preferred_element_type=jnp.float32
        )
        pairs[rows, pl.ds(0, DK)] = q
        weights[rows, :] = (scores * inside[...]).astype(jnp.bfloat16)
        decayed[rows, :] = (k.astype(jnp.float32) * key_decay[:, 0:1]).astype(jnp.bfloat16)


def retain_blocks(start, length, tables, gain, held, memory, head_out):
    pairs, weights, decayed, values = held
    inside, query_decay = tables[2], tables[3]
    block = inside.shape[-1]
    block_decay = head_rate(float(block), power=True)
    memory[...] = jnp.zeros_like(memory)

    @pl.loop(0, length // block)
    def _(b):
        rows = pl.ds(pl.multiple_of(start + b * block, block), block)
        v = values[rows, :]
        state = memory[...]
        kept = jnp.dot(weights[rows, :], v, preferred_element_type=jnp.float32) + query_decay[
            :, 0:1
        ] * jnp.dot(
            pairs[rows, pl.ds(0, DK)],
            state.astype(jnp.bfloat16),
            preferred_element_type=jnp.float32,
        )
        memory[...] = state * block_decay + lax.dot_general(
            decayed[rows, :], v, (((0,), (0,)), ((), ())), preferred_element_type=jnp.float32
        )
        scale = lax.rsqrt(jnp.mean(kept * kept, axis=-1, keepdims=True) + norm_eps)
        head_out[rows, :] = (kept * scale * gain[...]).astype(jnp.bfloat16)


def layer_kernel(depth, splits, along, *refs):
    args, refs = refs[:13], refs[13:]
    resid, mix_gain, query, key, value, head_gain, out_w, mlp_gain, gate, up, down, cos, sin = args
    out, refs = refs[0], refs[1:]
    fulls, others, refs = refs[:5], refs[5:10], refs[10:]
    pair_full, value_full, out_full, gate_up, down_full = fulls
    pair_other, value_other, out_other, gate_up_other, down_other = others
    x, gain_mix, gain_head, gain_mlp, cos_v, sin_v, middle_gate, middle_up, refs = (
        *refs[:8],
        refs[8:],
    )
    normed, both, pairs, values, weights, decayed, memory, head_out, hidden, refs = (
        *refs[:9],
        refs[9:],
    )
    part, sent, got, far_part, far_sent, far_got, far_sum, far_in, middle, refs = (
        *refs[:9],
        refs[9:],
    )
    inside, query_decay, key_decay, refs = *refs[:3], refs[3:]
    send_sem, recv_sem, cross_send, cross_recv, refs = *refs[:4], refs[4:]
    load_sem, peer_send, peer_recv, beside_send, beside_recv, out_sem = refs

    axes = (0, 0, 1, 0, 1)
    ga = Gather(
        depth,
        [Weight(*given) for given in zip(fulls, others, axes)],
        along,
        (cross_send, cross_recv),
        (send_sem, recv_sem),
    )
    peer = Near("tp", peer_send, peer_recv)
    beside = Near("fs", beside_send, beside_recv)
    core = lax.axis_index("tp")
    fs = lax.axis_index("fs")
    y = lax.rem(fs, 2)
    rows, width = x.shape
    units = gate.shape[1]
    whole = units // 2 // TILE
    aligned = whole * TILE
    step = aligned + TILE
    cols_of = down.shape[1]
    blocks = width // cols_of

    def own(w):
        weight = ga.weights[w]
        return ga.place(w, fs, 0, weight.rows)

    shard = query.shape[0]
    own_rows = pl.ds(pl.multiple_of(fs * shard, 16), shard)
    own_cols = pl.ds(pl.multiple_of(fs * cols_of, 128), cols_of)

    def heads(ref, side, size):
        return ref.at[:, pl.ds(pl.multiple_of(side * size, 128), size)]

    def down_pieces(side, place):
        rest = units // 2 - aligned
        return [
            (down.at[pl.ds(pl.multiple_of(side * step, 16), aligned), :], place(0, aligned)),
            (
                down.at[pl.ds(pl.multiple_of(aligned + side * rest, 16), rest), :],
                place(aligned, rest),
            ),
        ]

    moves = [
        (heads(query, y, DK), pair_full.at[own_rows, pl.ds(0, DK)]),
        (heads(key, y, DK), pair_full.at[own_rows, pl.ds(DK, DK)]),
        (heads(query, 1 - y, DK), pair_other.at[:, pl.ds(0, DK)]),
        (heads(key, 1 - y, DK), pair_other.at[:, pl.ds(DK, DK)]),
        (heads(value, y, DV), own(1)),
        (heads(value, 1 - y, DV), value_other),
        (resid, x),
        (mix_gain, gain_mix),
        (out_w.at[pl.ds(pl.multiple_of(y * DV, 16), DV), :], own(2)),
        (out_w.at[pl.ds(pl.multiple_of((1 - y) * DV, 16), DV), :], out_other),
        (gate.at[:, pl.ds(aligned, TILE)], middle_gate),
        (up.at[:, pl.ds(aligned, TILE)], middle_up),
        *down_pieces(y, lambda start, count: down_full.at[pl.ds(start, count), own_cols]),
        *down_pieces(1 - y, lambda start, count: down_other.at[pl.ds(start, count), :]),
        (cos, cos_v),
        (sin, sin_v),
        (heads(head_gain, y, DV), gain_head),
        (mlp_gain, gain_mlp),
    ]
    loads = [
        pltpu.make_async_copy(source, place, load_sem.at[i])
        for i, (source, place) in enumerate(moves)
    ]
    for load in loads[:10]:
        load.start()
    gathers = []
    for side, target, index in ((y, own(3), 0), (1 - y, gate_up_other, 1)):
        sem = load_sem.at[len(moves) + index]

        @pl.loop(0, whole)
        def _(j):
            cols = pl.ds(pl.multiple_of(side * step + j * TILE, TILE), TILE)
            for i, source in enumerate((gate, up)):
                place = pl.ds(pl.multiple_of(j * 2 * TILE, TILE) + i * TILE, TILE)
                pltpu.make_async_copy(source.at[:, cols], target.at[:, place], sem).start()

        bulk = target.at[:, pl.ds(0, 2 * aligned)]
        gathers.append(pltpu.make_async_copy(bulk, bulk, sem))
    for load in loads[10:]:
        load.start()

    ga.barrier()

    waited = set()

    def once(name, waits):
        if name not in waited:
            waited.add(name)
            for wait in waits:
                wait()

    def loaded(*indices):
        for i in indices:
            once(("load", i), [loads[i].wait])

    def side_of(far):
        return 1 - y if far else y

    def chip_rows(far, of):
        return pl.ds(pl.multiple_of((side_of(far) * 2 + of) * rows, 16), rows)

    def chip_start(far):
        return pl.multiple_of(side_of(far) * 2 * rows, 16)

    def tokens(far):
        return pl.ds(chip_start(far), 2 * rows)

    streams = (normed, both)
    starts = [sum(splits[:i]) for i in range(len(splits))]

    def rows_at(layer, far, of, i):
        start = pl.multiple_of((side_of(far) * 2 + of) * rows + starts[i], 16)
        return streams[layer].at[pl.ds(start, splits[i]), :]

    def join_own(layer, i, of):
        place = rows_at(layer, 0, of, i)
        return peer.copy(layer, i, place, place)

    def join_far(layer, i, of):
        place = rows_at(layer, 1, of, i)
        return peer.copy(layer, len(splits) + i, place, place)

    def join_beside(layer, i, far):
        place = rows_at(layer, far, core, i)
        return beside.copy(layer, i, place, place)

    def block_cols(block):
        return pl.ds(pl.multiple_of(block * cols_of, 128), cols_of)

    def share(layer, block):
        cols = block_cols(block)
        return peer.copy(layer, 2 * len(splits) + block, sent.at[:, cols], got.at[:, cols])

    def swap_far(layer, block):
        cols = block_cols(block)
        index = 2 * len(splits) + blocks + block
        return peer.copy(layer, index, far_sent.at[:, cols], far_got.at[:, cols])

    def give(layer, block):
        cols = block_cols(block)
        return beside.copy(layer, len(splits) + block, far_sum.at[:, cols], far_in.at[:, cols])

    def spread(layer, i):
        join_beside(layer, i, 0).start()
        join_own(layer, i, core).start()

    def norm_mix():
        loaded(6, 7)
        for i, count in enumerate(splits):

            @pl.loop(0, count // ROWS)
            def _(r):
                at = starts[i] + r * ROWS
                here = pl.ds(pl.multiple_of(at, ROWS), ROWS)
                there = pl.ds(pl.multiple_of((y * 2 + core) * rows + at, ROWS), ROWS)
                normed[there, :] = scaled_rows(x[here, :].astype(jnp.float32), gain_mix[...])

            spread(0, i)
        loaded(10, 11)
        half = TILE // 2
        low_gate = middle_gate[...].astype(jnp.float32)
        low_up = middle_up[...].astype(jnp.float32)
        first = jnp.concatenate([low_gate[:, :half], low_up[:, :half]], axis=1)
        second = jnp.concatenate([low_gate[:, half:], low_up[:, half:]], axis=1)
        end = pl.ds(2 * aligned, TILE)
        mine = jnp.where(y == 0, first, second)
        theirs = jnp.where(y == 0, second, first)
        gate_up[own_rows, end] = mine.astype(jnp.bfloat16)
        gate_up_other[:, end] = theirs.astype(jnp.bfloat16)
        make_tables(inside, query_decay, key_decay)

    ready = {
        0: (0, 1), 1: (2, 3), 2: (4,), 3: (5,), 4: (8,), 5: (9,), 6: (), 7: (), 8: (12, 13),
        9: (14, 15),
    }

    def prepared(s):
        loaded(*ready[s])
        if s in (6, 7):
            once(("gather", s), [gathers[s - 6].wait])

    def h(s, t):
        if t == 0 and s % 2 == 0:
            prepared(s)
        ga.arrive(s, t)

    def cross(s):
        prepared(s)
        ga.cross(s).start()

    def pass_on(layer, i):
        join_beside(layer, i, 1).wait_recv()
        join_far(layer, i, core).start()

    def gathered(w):
        once(
            ("weight", w),
            [
                functools.partial(ga.joined, 2 * w + far, rank)
                for rank in range(depth)
                for far in (0, 1)
            ],
        )

    def arrived(layer, far, i):
        join = join_far if far else join_own
        once(("rows", layer, far, i), [lambda: join(layer, i, 1 - core).wait_recv()])

    def project(w, far, place):
        gathered(w)
        for i in range(len(splits)):
            arrived(0, far, i)
        here = tokens(far)
        full = fulls[w]

        @pl.loop(0, full.shape[1] // 256)
        def _(c):
            cols = pl.ds(pl.multiple_of(c * 256, 256), 256)
            place[here, cols] = jnp.dot(
                normed[here, :], full[:, cols], preferred_element_type=jnp.float32
            ).astype(jnp.bfloat16)

    tables = (cos_v, sin_v, inside, query_decay, key_decay)

    def pairs_of(far):
        project(0, far, pairs)
        loaded(16, 17)
        weigh_blocks(chip_start(far), 2 * rows, tables, pairs, weights, decayed)

    def values_of(far):
        project(1, far, values)

    def retain(far):
        loaded(18, 19)
        held = (pairs, weights, decayed, values)
        retain_blocks(chip_start(far), 2 * rows, tables, gain_head, held, memory, head_out)

    lefts, rights = (head_out, hidden), (out_full, down_full)

    def product(layer, far, of, block, place):
        cols = block_cols(block)
        place[:, cols] = jnp.dot(
            lefts[layer][chip_rows(far, of), :],
            rights[layer][:, cols],
            preferred_element_type=jnp.float32,
        ).astype(jnp.bfloat16)

    def far_rank(layer, rank):
        origin = ga.near(rank)
        for far in (0, 1):
            ga.joined((4, 8)[layer] + far, rank)
            block = ga.block(far, origin)
            if layer == 1:
                swap_far(0, block).wait_send()
                give(0, block).wait_send()
            product(layer, 1, 1 - core, block, far_sent)
            swap_far(layer, block).start()
            product(layer, 1, core, block, far_part)
        for far in (0, 1):
            block = ga.block(far, origin)
            cols = block_cols(block)
            swap_far(layer, block).wait_recv()
            total = far_part[:, cols].astype(jnp.float32) + far_got[:, cols].astype(jnp.float32)
            far_sum[:, cols] = total.astype(jnp.bfloat16)
            give(layer, block).start()

    def own_rank(layer, rank):
        for far in (0, 1):
            block = ga.block(far, ga.near(rank))
            product(layer, 0, 1 - core, block, sent)
            share(layer, block).start()
            product(layer, 0, core, block, part)

    def norm_mlp():
        for block in range(blocks):
            share(0, block).wait()
        for block in range(blocks):
            give(0, block).wait_recv()
        for i, count in enumerate(splits):

            @pl.loop(0, count // ROWS)
            def _(r):
                at = starts[i] + r * ROWS
                here = pl.ds(pl.multiple_of(at, ROWS), ROWS)
                there = pl.ds(pl.multiple_of((y * 2 + core) * rows + at, ROWS), ROWS)
                total = part[here, :].astype(jnp.float32) + got[here, :].astype(jnp.float32)
                total = total + far_in[here, :].astype(jnp.float32)
                mid = (x[here, :].astype(jnp.float32) + total).astype(jnp.bfloat16)
                middle[here, :] = mid
                both[there, :] = scaled_rows(mid.astype(jnp.float32), gain_mlp[...])

            spread(1, i)

    def activate(ranges):
        @pl.loop(0, whole)
        def _(j):
            cols = pl.ds(pl.multiple_of(j * 2 * TILE, 2 * TILE), 2 * TILE)
            place = pl.ds(pl.multiple_of(j * TILE, TILE), TILE)
            for here in ranges:
                two = jnp.dot(both[here, :], gate_up[:, cols], preferred_element_type=jnp.float32)
                hidden[here, place] = (jax.nn.silu(two[:, :TILE]) * two[:, TILE:]).astype(
                    jnp.bfloat16
                )

        half = TILE // 2
        for here in ranges:
            two = jnp.dot(
                both[here, :],
                gate_up[:, pl.ds(2 * aligned, TILE)],
                preferred_element_type=jnp.float32,
            )
            hidden[here, pl.ds(aligned, half)] = (
                jax.nn.silu(two[:, :half]) * two[:, half:]
            ).astype(jnp.bfloat16)

    def expand(far, i=None):
        gathered(3)
        if far:
            arrived(1, 1, i)
            activate(
                [
                    pl.ds(
                        pl.multiple_of((side_of(1) * 2 + of) * rows + starts[i], 16), splits[i]
                    )
                    for of in (0, 1)
                ]
            )
        else:
            for part_index in range(len(splits)):
                arrived(1, 0, part_index)
            activate([tokens(0)])

    def finish():
        for block in range(blocks):
            share(1, block).wait()
        writes = []
        for rank in range(depth):
            origin = ga.near(rank)
            for far in (1, 0):
                block = ga.block(far, origin)
                cols = block_cols(block)
                give(1, block).wait_recv()
                total = part[:, cols].astype(jnp.float32) + got[:, cols].astype(jnp.float32)
                total = total + far_in[:, cols].astype(jnp.float32)
                middle[:, cols] = (middle[:, cols].astype(jnp.float32) + total).astype(
                    jnp.bfloat16
                )
                write = pltpu.make_async_copy(
                    middle.at[:, cols], out.at[:, cols], out_sem.at[block]
                )
                write.start()
                writes.append(write)
        for write in writes:
            write.wait()

    order = [
        (h, 2, 0), (h, 0, 0), (cross, 3), (cross, 1), (norm_mix,), (cross, 5), (h, 3, 0),
        (h, 2, 1), (h, 1, 0), (h, 2, 2), (h, 1, 1), (h, 2, 3), (h, 3, 1), (cross, 9), (h, 0, 1),
        (h, 3, 2), (h, 0, 2), (pass_on, 0, 0), (h, 4, 0), (h, 3, 3), (h, 1, 2), (h, 1, 3),
        (h, 0, 3), (h, 6, 0), (pass_on, 0, 1), (values_of, 0), (h, 5, 0), (cross, 7),
        (values_of, 1), (h, 4, 1), (pairs_of, 1), (retain, 1), (h, 5, 1), (far_rank, 0, 0),
        (h, 4, 2), (pairs_of, 0), (h, 5, 2), (far_rank, 0, 1), (h, 6, 1), (h, 4, 3), (retain, 0),
        (h, 5, 3), (far_rank, 0, 2), (h, 7, 0), (far_rank, 0, 3), (h, 6, 2), (own_rank, 0, 3),
        (h, 7, 1), (own_rank, 0, 2), (own_rank, 0, 1), (own_rank, 0, 0), (h, 9, 0), (norm_mlp,),
        (h, 6, 3), (h, 7, 2), (h, 7, 3), (h, 9, 1), (h, 8, 0), (pass_on, 1, 0), (h, 8, 1),
        (h, 9, 2), (expand, 1, 0), (pass_on, 1, 1), (h, 8, 2), (h, 9, 3), (expand, 1, 1),
        (far_rank, 1, 1), (far_rank, 1, 0), (expand, 0), (h, 8, 3), (own_rank, 1, 1),
        (far_rank, 1, 2), (own_rank, 1, 0), (own_rank, 1, 2), (far_rank, 1, 3), (own_rank, 1, 3),
        (finish,),
    ]
    for job, *given in order:
        job(*given)
    for s in range(2 * len(fulls)):
        ga.drain(s)
    for layer in (0, 1):
        for i in range(len(splits)):
            join_own(layer, i, core).wait_send()
            join_far(layer, i, core).wait_send()
            join_beside(layer, i, 0).wait_send()
    for block in range(blocks):
        swap_far(1, block).wait_send()
        give(1, block).wait_send()


def rotation_tables(length_total, half_width):
    position = np.arange(length_total, dtype=np.float32)
    inverse = (1.0 / rope_base ** np.linspace(0.0, 1.0, half_width)).astype(np.float32)
    angle = (position[:, None] * inverse[None, :]).astype(np.float64)
    return np.cos(angle).astype(np.float32), np.sin(angle).astype(np.float32)


def fits(rows, width, key_cols, value_cols, units, shard, out_cols):
    axes = lax.axis_size("rep") == 2 and lax.axis_size("fs") == 8 and lax.axis_size("tp") == 2
    cut = units % (2 * TILE) == TILE and (units // 2) % 32 == 0
    whole = width == 8 * out_cols and width == 8 * shard and shard % 256 == 0
    heads = key_cols == 2 * DK and value_cols == 2 * DV
    return axes and cut and whole and heads and rows % 192 == 0


def layer(args):
    resid, query, gate, down = args[0], args[2], args[8], args[10]
    size = lax.axis_size("fs")
    depth = size // 2
    rows, width = resid.shape
    tokens = 4 * rows
    units = gate.shape[1]
    shard, out_cols = query.shape[0], down.shape[1]
    others = [(shard, 2 * DK), (shard, DV), (DV, out_cols), (shard, units), (units // 2, out_cols)]
    fulls = []
    for (r, c), axis in zip(others, (0, 0, 1, 0, 1)):
        fulls.append((r * size, c) if axis == 0 else (r, c * size))
    along = [shard // 2, shard // 2, DV // 2, shard // 16 * 9 // 16 * 16, units // 2 // 2]
    splits = (2 * rows // 3, rows // 3)
    cosine, sine = rotation_tables(2 * rows, DK // 2)
    far = pl.BlockSpec(memory_space=pl.ANY)
    bf, f32 = jnp.bfloat16, jnp.float32
    vm = pltpu.VMEM
    dma = pltpu.SemaphoreType.DMA
    slices = 2 * len(fulls)
    peers = 2 * len(splits) + 2 * size
    args = [a[None, :] if a.ndim == 1 else a for a in args]
    return pl.pallas_call(
        functools.partial(layer_kernel, depth, splits, along),
        out_shape=jax.ShapeDtypeStruct((rows, width), bf),
        in_specs=[far] * 13,
        out_specs=far,
        scratch_shapes=[vm(s, bf) for s in fulls]
        + [vm(s, bf) for s in others]
        + [
            vm((rows, width), bf),
            vm(args[1].shape, f32),
            vm((1, DV), f32),
            vm(args[7].shape, f32),
            vm(cosine.shape, f32),
            vm(sine.shape, f32),
            vm((shard, TILE), bf),
            vm((shard, TILE), bf),
            vm((tokens, width), bf),
            vm((tokens, width), bf),
            vm((tokens, 2 * DK), bf),
            vm((tokens, DV), bf),
            vm((tokens, BLOCK), bf),
            vm((tokens, DK), bf),
            vm((DK, DV), f32),
            vm((tokens, DV), bf),
            vm((tokens, units // 2), bf),
        ]
        + [vm((rows, width), bf)] * 9
        + [vm((BLOCK, BLOCK), f32)] * 3
        + [
            dma((slices, 3, depth)),
            dma((slices, 2, depth)),
            dma((len(fulls),)),
            dma((len(fulls),)),
            dma((22,)),
            dma((2, peers)),
            dma((2, peers)),
            dma((2, len(splits) + size)),
            dma((2, len(splits) + size)),
            dma((size,)),
        ],
        compiler_params=pltpu.CompilerParams(
            collective_id=0, has_side_effects=True, vmem_limit_bytes=67043328
        ),
    )(*args, jnp.asarray(cosine), jnp.asarray(sine))


DK = 256
DV = 512
BLOCK = 128


norm_eps = 1e-06
rope_base = 10000.0


def rms_scale(values, gain):
    widened = values.astype(jnp.float32)
    scaled = widened * lax.rsqrt(jnp.mean(widened * widened, axis=-1, keepdims=True) + norm_eps)
    return (scaled * gain).astype(jnp.bfloat16)


def rotation(length_total, half_width):
    position = jnp.arange(length_total, dtype=jnp.float32)
    inverse = 1.0 / rope_base ** jnp.linspace(0.0, 1.0, half_width, dtype=jnp.float32)
    angle = position[:, None] * inverse[None, :]
    return (jnp.cos(angle), jnp.sin(angle))


def rotate(vectors):
    length_total = vectors.shape[0]
    half_width = vectors.shape[-1] // 2
    cosine, sine = rotation(length_total, half_width)
    cosine, sine = cosine[:, None, :], sine[:, None, :]
    first = vectors[..., :half_width]
    second = vectors[..., half_width:]
    return jnp.concatenate(
        [first * cosine - second * sine, second * cosine + first * sine], axis=-1
    )


def decay_tables(head_ids, block):
    log_gamma = jnp.log1p(-(2.0 ** (-5.0 - 2.0 * head_ids.astype(jnp.float32))))
    offset = jnp.arange(block, dtype=jnp.float32)
    distance = offset[:, None] - offset[None, :]
    inside = jnp.where(
        distance >= 0, jnp.exp(log_gamma[:, None, None] * jnp.maximum(distance, 0.0)), 0.0
    )
    query_decay = jnp.exp(log_gamma[:, None] * (offset + 1.0))
    key_decay = jnp.exp(log_gamma[:, None] * (block - 1.0 - offset))
    block_decay = jnp.exp(log_gamma * block)
    return (inside, query_decay, key_decay, block_decay)


def retain(queries, keys, values, head_ids, block):
    length_total, heads, key_width = queries.shape
    value_width = values.shape[-1]
    count = length_total // block
    inside, query_decay, key_decay, block_decay = decay_tables(head_ids, block)

    def blocks(tensor):
        return tensor.reshape(count, block, heads, tensor.shape[-1]).transpose(0, 2, 1, 3)

    def advance(memory, inputs):
        query_tile_rows, key_tile_rows, value_block = inputs
        attention_scores = jnp.einsum(
            "zvf,zjf->zvj", query_tile_rows, key_tile_rows, preferred_element_type=jnp.float32
        )
        weights = (attention_scores * inside).astype(jnp.bfloat16)
        within = jnp.einsum(
            "hlm,hmv->hlv", weights, value_block, preferred_element_type=jnp.float32
        )
        carried = (
            jnp.einsum(
                "hld,hdv->hlv",
                query_tile_rows,
                memory.astype(jnp.bfloat16),
                preferred_element_type=jnp.float32,
            )
            * query_decay[:, :, None]
        )
        weighted_keys = (key_tile_rows.astype(jnp.float32) * key_decay[:, :, None]).astype(
            jnp.bfloat16
        )
        memory = memory * block_decay[:, None, None] + jnp.einsum(
            "hld,hlv->hdv", weighted_keys, value_block, preferred_element_type=jnp.float32
        )
        return (memory, within + carried)

    start_state = jnp.zeros((heads, key_width, value_width), jnp.float32)
    _, outputs = lax.scan(advance, start_state, (blocks(queries), blocks(keys), blocks(values)))
    return outputs.transpose(0, 2, 1, 3).reshape(length_total, heads, value_width)


def head_scale(retained, gain):
    scaled = retained * lax.rsqrt(jnp.mean(retained * retained, axis=-1, keepdims=True) + norm_eps)
    return (scaled.reshape(retained.shape[0], -1) * gain).astype(jnp.bfloat16)


def swap(rows):
    return lax.ppermute(rows, "tp", [(0, 1), (1, 0)])


def join_rows(rows):
    if lax.axis_size("tp") != 2:
        return lax.all_gather(rows, "tp", axis=0, tiled=True)
    first = lax.axis_index("tp") == 0
    got = swap(rows)
    return jnp.concatenate([jnp.where(first, rows, got), jnp.where(first, got, rows)], axis=0)


def share_sum(part):
    if lax.axis_size("tp") != 2:
        summed = lax.psum_scatter(part, "tp", scatter_dimension=0, tiled=True)
        return summed.astype(jnp.float32)
    count = part.shape[0] // 2
    me = lax.axis_index("tp")
    mine = lax.dynamic_slice_in_dim(part, me * count, count, axis=0)
    theirs = lax.dynamic_slice_in_dim(part, (1 - me) * count, count, axis=0)
    return mine.astype(jnp.float32) + swap(theirs).astype(jnp.float32)


def shards(
    resid,
    mix_gain,
    query_weight,
    key_weight,
    value_weight,
    head_gain,
    out_weight,
    mlp_gain,
    gate_weight,
    up_weight,
    down_weight,
):
    token_rows = resid.shape[0]
    length_total = token_rows * lax.axis_size("tp")
    key_cols = query_weight.shape[1]
    heads_here = key_cols // DK
    sizes = (
        token_rows, resid.shape[1], key_cols, value_weight.shape[1], gate_weight.shape[1],
        query_weight.shape[0], down_weight.shape[1],
    )
    if fits(*sizes):
        args = [
            resid, mix_gain, query_weight, key_weight, value_weight, head_gain,
            out_weight, mlp_gain, gate_weight, up_weight, down_weight,
        ]
        return layer(args)
    normed = rms_scale(resid, mix_gain)
    mixer_shard = jnp.concatenate([query_weight, key_weight, value_weight], axis=1)
    mlp_shard = jnp.concatenate([gate_weight, up_weight], axis=1)
    normed_full = join_rows(normed)
    head_ids = lax.axis_index("tp") * heads_here + jnp.arange(heads_here, dtype=jnp.int32)
    pieces = [mixer_shard, out_weight, mlp_shard, down_weight]
    mixer_full, out_full, mlp_full, down_full = (
        lax.all_gather(s, "fs", axis=a, tiled=True) for s, a in zip(pieces, [0, 1, 0, 1])
    )
    projected = jnp.dot(
        normed_full, mixer_full, preferred_element_type=jnp.float32
    ).astype(jnp.bfloat16)
    both_keys = projected[:, : 2 * key_cols].astype(jnp.float32)
    both_keys = both_keys.reshape(length_total, 2, heads_here, DK)
    values = projected[:, 2 * key_cols :].reshape(length_total, heads_here, DV)
    query_rot = rotate(both_keys[:, 0]).astype(jnp.bfloat16)
    key_rot = (rotate(both_keys[:, 1]) * DK ** (-0.5)).astype(jnp.bfloat16)
    retained = retain(query_rot, key_rot, values, head_ids, BLOCK)
    head_out = head_scale(retained, head_gain)
    part = jnp.dot(head_out, out_full, preferred_element_type=jnp.float32).astype(jnp.bfloat16)
    mixer_sum = share_sum(part)
    middle = (resid.astype(jnp.float32) + mixer_sum).astype(jnp.bfloat16)
    normed_mlp = rms_scale(middle, mlp_gain)
    local_units = gate_weight.shape[1]
    both = jnp.dot(
        join_rows(normed_mlp),
        mlp_full,
        preferred_element_type=jnp.float32,
    )
    hidden_units = (jax.nn.silu(both[:, :local_units]) * both[:, local_units:]).astype(jnp.bfloat16)
    mlp_sum = share_sum(
        jnp.dot(hidden_units, down_full, preferred_element_type=jnp.float32).astype(jnp.bfloat16)
    )
    return (middle.astype(jnp.float32) + mlp_sum).astype(jnp.bfloat16)


def solution(mesh):
    placed = (
        P(("rep", "fs", "tp"), None),
        P(),
        P("fs", "tp"),
        P("fs", "tp"),
        P("fs", "tp"),
        P("tp"),
        P("tp", "fs"),
        P(),
        P("fs", "tp"),
        P("fs", "tp"),
        P("tp", "fs"),
    )
    return jax.shard_map(
        shards, mesh=mesh, in_specs=placed, out_specs=P(("rep", "fs", "tp"), None), check_vma=False
    )
```

time: 296 us -> 181 us (0.61)
  Pallas kernels: 236 us -> 178 us
  other arithmetic: 22.6 us -> 0 us
  matrix products: 21.3 us -> 0 us
  waiting for transfers between devices: 10.1 us -> 0 us
    pallas_call x1, Pallas kernels: 236 us -> 178 us  [layer(): pl.pallas_call(functools.partial(layer_kernel, depth, splits, along), out...]
    dot_general x2 -> x0, matrix products: 21.3 us -> none  [the longest x1 12.5 us: shards(): jnp.dot(join_rows(normed_mlp), mlp_full, preferred_element_type=jnp.float32)]
    ppermute x4 -> x0, waiting for transfers between devices: 10.1 us -> none  [swap(): return lax.ppermute(rows, 'tp', [(0, 1), (1, 0)])]
    concatenate x3 -> x0, other arithmetic: 6.8 us -> none  [the longest x1 2.58 us: shards(): mlp_shard = jnp.concatenate([gate_weight, up_weight], axis=1)]
    convert_element_type x3 -> x0, other arithmetic: 5.39 us -> none  [the longest x2 3.41 us: rms_scale(): return (scaled * gain).astype(jnp.bfloat16)]
    reduce_sum x2 -> x0, other arithmetic: 4.34 us -> none  [rms_scale(): jnp.mean(widened * widened, axis=-1, keepdims=True) + norm_eps]
  transfers between devices with their start and end apart: 4 -> 0, of which waited for: 3 -> 0; matrix products, arithmetic and copies ran while one was open for 3% -> 0% of each run, Pallas kernels for 0% -> 0%
where the time goes in v3:
time: 181 us
  Pallas kernels  178 us (98%)
  local copies, waits for them, and re-layouts  2.73 us (2%)
    pallas_call x1, Pallas kernels, layer(): pl.pallas_call(functools.partial(layer_kernel, depth, splits, along), out...  178 us

profile of v3, /device:TPU:0, one launch (start us, length us, event | category | flops | bytes accessed | tf_op | source)
XLA Modules:
  0.0 180.7 jit_solution(12465966513733962943)
XLA Ops:
  0.0 177.9 %shard_map.127 = bf16[384,2048]{1,0:T(8,128)(2,1)} custom-call(bf16[384,2048]{1,0:T(8,128)(2,1)} %refs_0_.1, f32[1,2048]{1,0:T(1,128)} %bitcast.3, bf16[256,512]{1,0:T(8,128)(2,1)} %refs_2_.1, bf16[256,512]{1,0:T(8,128)(2,1)} %refs_3_.1, bf16[256,1024]{1,0:T(8,128)(2,1)} %refs_4_.1, f32[1,1024]{1,0:T(1,128)} %bitcast.5, bf16[1024,256]{1,0:T(8,128)(2,1)} %refs_6_.1, ...), custom_call_target="tpu_custom_call" | custom-call | tf_op jit(solution)/shard_map/pallas_call | solution.py:718
  177.9 2.7 %copy.15 = bf16[384,2048]{1,0:T(8,128)(2,1)} copy(bf16[384,2048]{1,0:T(8,128)(2,1)} %shard_map.127) | data formatting | bytes 3145728

commit v4 on v3

--- a/solution.py
+++ b/solution.py
@@ -30,7 +30,7 @@
         self.z = fs // 2
         self.y = lax.rem(fs, 2)
 
-    def barrier(self):
+    def greet(self):
         sem = pltpu.get_barrier_semaphore()
         z, y, x = self.z, self.y, self.x
         core = lax.axis_index("tp")
@@ -46,9 +46,10 @@
         def _():
             pl.semaphore_signal(sem, inc=1, device_id={"fs": (z + 1) * 2 + y}, device_id_type=MESH)
 
-        low = jnp.minimum(z, 1)
-        high = jnp.minimum(self.depth - 1 - z, 1)
-        pl.semaphore_wait(sem, 3 + low + high)
+    def meet(self):
+        low = jnp.minimum(self.z, 1)
+        high = jnp.minimum(self.depth - 1 - self.z, 1)
+        pl.semaphore_wait(pltpu.get_barrier_semaphore(), 3 + low + high)
 
     def near(self, rank):
         place = 0
@@ -82,7 +83,7 @@
             device_id_type=MESH,
         )
 
-    def copy(self, s, kind, origin, incoming=False):
+    def copy(self, s, kind, origin, incoming=False, own=False):
         w, far = s // 2, s % 2
         x, y, z = self.x, self.y, self.z
         rows, along = self.weights[w].rows, self.along[w]
@@ -98,13 +99,16 @@
             "x": {"rep": 1 - x},
         }[kind]
         place = self.place(w, self.block(far, origin), start, count)
-        sends = ("up", "down", "x").index(kind)
-        receives = (0, 0, 1)[sends]
+        slot = origin
+        if kind == "x":
+            slot = self.depth + origin
+        elif kind == "down" and own:
+            slot = 2 * self.depth
         return pltpu.make_async_remote_copy(
             src_ref=place,
             dst_ref=place,
-            send_sem=self.send_sem.at[s, sends, origin],
-            recv_sem=self.recv_sem.at[s, receives, origin],
+            send_sem=self.send_sem.at[s, slot],
+            recv_sem=self.recv_sem.at[s, origin + (self.depth if kind == "x" else 0)],
             device_id=target,
             device_id_type=MESH,
         )
@@ -133,7 +137,7 @@
 
             @pl.when(self.z > 0)
             def _():
-                act(self.copy(s, "down", origin))
+                act(self.copy(s, "down", origin, own=way == "own"))
 
     def arrive(self, s, t):
         def body(way, origin):
@@ -173,12 +177,12 @@
             fs = lax.axis_index("fs")
             self.target = {"fs": fs // 2 * 2 + 1 - lax.rem(fs, 2)}
 
-    def copy(self, layer, index, source, place):
+    def copy(self, index, source, place):
         return pltpu.make_async_remote_copy(
             src_ref=source,
             dst_ref=place,
-            send_sem=self.send_sem.at[layer, index],
-            recv_sem=self.recv_sem.at[layer, index],
+            send_sem=self.send_sem.at[index],
+            recv_sem=self.recv_sem.at[index],
             device_id=self.target,
             device_id_type=MESH,
         )
@@ -289,7 +293,7 @@
     )
     inside, query_decay, key_decay, refs = *refs[:3], refs[3:]
     send_sem, recv_sem, cross_send, cross_recv, refs = *refs[:4], refs[4:]
-    load_sem, peer_send, peer_recv, beside_send, beside_recv, out_sem = refs
+    load_sem, peer_send, peer_recv, beside_send, beside_recv = refs
 
     axes = (0, 0, 1, 0, 1)
     ga = Gather(
@@ -299,6 +303,7 @@
         (cross_send, cross_recv),
         (send_sem, recv_sem),
     )
+    ga.greet()
     peer = Near("tp", peer_send, peer_recv)
     beside = Near("fs", beside_send, beside_recv)
     core = lax.axis_index("tp")
@@ -310,7 +315,6 @@
     aligned = whole * TILE
     step = aligned + TILE
     cols_of = down.shape[1]
-    blocks = width // cols_of
 
     def own(w):
         weight = ga.weights[w]
@@ -357,25 +361,29 @@
         pltpu.make_async_copy(source, place, load_sem.at[i])
         for i, (source, place) in enumerate(moves)
     ]
-    for load in loads[:10]:
+    for load in loads[:8]:
         load.start()
     gathers = []
-    for side, target, index in ((y, own(3), 0), (1 - y, gate_up_other, 1)):
-        sem = load_sem.at[len(moves) + index]
-
-        @pl.loop(0, whole)
-        def _(j):
-            cols = pl.ds(pl.multiple_of(side * step + j * TILE, TILE), TILE)
-            for i, source in enumerate((gate, up)):
-                place = pl.ds(pl.multiple_of(j * 2 * TILE, TILE) + i * TILE, TILE)
-                pltpu.make_async_copy(source.at[:, cols], target.at[:, place], sem).start()
-
-        bulk = target.at[:, pl.ds(0, 2 * aligned)]
-        gathers.append(pltpu.make_async_copy(bulk, bulk, sem))
-    for load in loads[10:]:
-        load.start()
-
-    ga.barrier()
+
+    def load_rest():
+        for load in loads[8:12]:
+            load.start()
+        for side, target, index in ((y, own(3), 0), (1 - y, gate_up_other, 1)):
+            sem = load_sem.at[len(moves) + index]
+
+            @pl.loop(0, whole)
+            def _(j):
+                cols = pl.ds(pl.multiple_of(side * step + j * TILE, TILE), TILE)
+                for i, source in enumerate((gate, up)):
+                    place = pl.ds(pl.multiple_of(j * 2 * TILE, TILE) + i * TILE, TILE)
+                    pltpu.make_async_copy(source.at[:, cols], target.at[:, place], sem).start()
+
+            bulk = target.at[:, pl.ds(0, 2 * aligned)]
+            gathers.append(pltpu.make_async_copy(bulk, bulk, sem))
+        for load in loads[12:]:
+            load.start()
+
+    ga.meet()
 
     waited = set()
 
@@ -410,37 +418,42 @@
 
     def join_own(layer, i, of):
         place = rows_at(layer, 0, of, i)
-        return peer.copy(layer, i, place, place)
+        return peer.copy(i, place, place)
 
     def join_far(layer, i, of):
         place = rows_at(layer, 1, of, i)
-        return peer.copy(layer, len(splits) + i, place, place)
+        return peer.copy(len(splits) + i, place, place)
 
     def join_beside(layer, i, far):
         place = rows_at(layer, far, core, i)
-        return beside.copy(layer, i, place, place)
-
-    def block_cols(block):
-        return pl.ds(pl.multiple_of(block * cols_of, 128), cols_of)
-
-    def share(layer, block):
-        cols = block_cols(block)
-        return peer.copy(layer, 2 * len(splits) + block, sent.at[:, cols], got.at[:, cols])
-
-    def swap_far(layer, block):
-        cols = block_cols(block)
-        index = 2 * len(splits) + blocks + block
-        return peer.copy(layer, index, far_sent.at[:, cols], far_got.at[:, cols])
-
-    def give(layer, block):
-        cols = block_cols(block)
-        return beside.copy(layer, len(splits) + block, far_sum.at[:, cols], far_in.at[:, cols])
+        return beside.copy(i, place, place)
+
+    def wide(rank):
+        return pl.ds(pl.multiple_of(ga.near(rank) * 2 * cols_of, 128), 2 * cols_of)
+
+    def part_rows(i):
+        return pl.ds(starts[i], splits[i])
+
+    def share(rank):
+        cols = wide(rank)
+        return peer.copy(2 * len(splits) + rank, sent.at[:, cols], got.at[:, cols])
+
+    def swap_far(rank, i):
+        here, cols = part_rows(i), wide(rank)
+        index = 2 * len(splits) + (1 + i) * depth + rank
+        return peer.copy(index, far_sent.at[here, cols], far_got.at[here, cols])
+
+    def give(rank, i):
+        here, cols = part_rows(i), wide(rank)
+        index = len(splits) + i * depth + rank
+        return beside.copy(index, far_sum.at[here, cols], far_in.at[here, cols])
 
     def spread(layer, i):
         join_beside(layer, i, 0).start()
         join_own(layer, i, core).start()
 
     def norm_mix():
+        load_rest()
         loaded(6, 7)
         for i, count in enumerate(splits):
 
@@ -486,6 +499,8 @@
 
     def pass_on(layer, i):
         join_beside(layer, i, 1).wait_recv()
+        if layer == 1:
+            join_far(0, i, core).wait_send()
         join_far(layer, i, core).start()
 
     def gathered(w):
@@ -502,29 +517,41 @@
         join = join_far if far else join_own
         once(("rows", layer, far, i), [lambda: join(layer, i, 1 - core).wait_recv()])
 
-    def project(w, far, place):
+    def far_span(of, i):
+        return pl.ds(pl.multiple_of((side_of(1) * 2 + of) * rows + starts[i], 16), splits[i])
+
+    def spans(layer, far, i):
+        if far:
+            arrived(layer, 1, i)
+            return [far_span(of, i) for of in (0, 1)]
+        for part in range(len(splits)):
+            arrived(layer, 0, part)
+        return [tokens(0)]
+
+    def project(w, far, i, place):
         gathered(w)
-        for i in range(len(splits)):
-            arrived(0, far, i)
-        here = tokens(far)
+        ranges = spans(0, far, i)
         full = fulls[w]
 
         @pl.loop(0, full.shape[1] // 256)
         def _(c):
             cols = pl.ds(pl.multiple_of(c * 256, 256), 256)
-            place[here, cols] = jnp.dot(
-                normed[here, :], full[:, cols], preferred_element_type=jnp.float32
-            ).astype(jnp.bfloat16)
+            for here in ranges:
+                place[here, cols] = jnp.dot(
+                    normed[here, :], full[:, cols], preferred_element_type=jnp.float32
+                ).astype(jnp.bfloat16)
 
     tables = (cos_v, sin_v, inside, query_decay, key_decay)
 
-    def pairs_of(far):
-        project(0, far, pairs)
+    def pairs_of(far, i=None):
+        project(0, far, i, pairs)
+
+    def values_of(far, i=None):
+        project(1, far, i, values)
+
+    def weigh(far):
         loaded(16, 17)
         weigh_blocks(chip_start(far), 2 * rows, tables, pairs, weights, decayed)
-
-    def values_of(far):
-        project(1, far, values)
 
     def retain(far):
         loaded(18, 19)
@@ -533,59 +560,61 @@
 
     lefts, rights = (head_out, hidden), (out_full, down_full)
 
-    def product(layer, far, of, block, place):
-        cols = block_cols(block)
-        place[:, cols] = jnp.dot(
-            lefts[layer][chip_rows(far, of), :],
-            rights[layer][:, cols],
-            preferred_element_type=jnp.float32,
-        ).astype(jnp.bfloat16)
-
-    def far_rank(layer, rank):
-        origin = ga.near(rank)
+    def product(layer, taken, rank, place, here):
+        for i in range(2):
+            start = pl.multiple_of((ga.near(rank) * 2 + i) * cols_of, 128)
+            cols = pl.ds(start, cols_of)
+            place[here, cols] = jnp.dot(
+                lefts[layer][taken, :], rights[layer][:, cols], preferred_element_type=jnp.float32
+            ).astype(jnp.bfloat16)
+
+    def rank_joined(layer, rank):
         for far in (0, 1):
-            ga.joined((4, 8)[layer] + far, rank)
-            block = ga.block(far, origin)
-            if layer == 1:
-                swap_far(0, block).wait_send()
-                give(0, block).wait_send()
-            product(layer, 1, 1 - core, block, far_sent)
-            swap_far(layer, block).start()
-            product(layer, 1, core, block, far_part)
-        for far in (0, 1):
-            block = ga.block(far, origin)
-            cols = block_cols(block)
-            swap_far(layer, block).wait_recv()
-            total = far_part[:, cols].astype(jnp.float32) + far_got[:, cols].astype(jnp.float32)
-            far_sum[:, cols] = total.astype(jnp.bfloat16)
-            give(layer, block).start()
+            s = (4, 8)[layer] + far
+            once(("rank", s, rank), [functools.partial(ga.joined, s, rank)])
+
+    def far_rank(layer, rank, i):
+        here, cols = part_rows(i), wide(rank)
+        rank_joined(layer, rank)
+        if layer == 1:
+            swap_far(rank, i).wait_send()
+            give(rank, i).wait_send()
+        product(layer, far_span(1 - core, i), rank, far_sent, here)
+        swap_far(rank, i).start()
+        product(layer, far_span(core, i), rank, far_part, here)
+        swap_far(rank, i).wait_recv()
+        total = far_part[here, cols].astype(jnp.float32) + far_got[here, cols].astype(jnp.float32)
+        far_sum[here, cols] = total.astype(jnp.bfloat16)
+        give(rank, i).start()
 
     def own_rank(layer, rank):
-        for far in (0, 1):
-            block = ga.block(far, ga.near(rank))
-            product(layer, 0, 1 - core, block, sent)
-            share(layer, block).start()
-            product(layer, 0, core, block, part)
-
-    def norm_mlp():
-        for block in range(blocks):
-            share(0, block).wait()
-        for block in range(blocks):
-            give(0, block).wait_recv()
-        for i, count in enumerate(splits):
-
-            @pl.loop(0, count // ROWS)
-            def _(r):
-                at = starts[i] + r * ROWS
-                here = pl.ds(pl.multiple_of(at, ROWS), ROWS)
-                there = pl.ds(pl.multiple_of((y * 2 + core) * rows + at, ROWS), ROWS)
-                total = part[here, :].astype(jnp.float32) + got[here, :].astype(jnp.float32)
-                total = total + far_in[here, :].astype(jnp.float32)
-                mid = (x[here, :].astype(jnp.float32) + total).astype(jnp.bfloat16)
-                middle[here, :] = mid
-                both[there, :] = scaled_rows(mid.astype(jnp.float32), gain_mlp[...])
-
-            spread(1, i)
+        everything = pl.ds(0, rows)
+        rank_joined(layer, rank)
+        product(layer, chip_rows(0, 1 - core), rank, sent, everything)
+        share(rank).start()
+        product(layer, chip_rows(0, core), rank, part, everything)
+
+    def norm_mlp(i):
+        if i == 0:
+            for rank in range(depth):
+                share(rank).wait()
+        for rank in range(depth):
+            give(rank, i).wait_recv()
+        join_beside(0, i, 0).wait_send()
+        join_own(0, i, core).wait_send()
+
+        @pl.loop(0, splits[i] // ROWS)
+        def _(r):
+            at = starts[i] + r * ROWS
+            here = pl.ds(pl.multiple_of(at, ROWS), ROWS)
+            there = pl.ds(pl.multiple_of((y * 2 + core) * rows + at, ROWS), ROWS)
+            total = part[here, :].astype(jnp.float32) + got[here, :].astype(jnp.float32)
+            total = total + far_in[here, :].astype(jnp.float32)
+            mid = (x[here, :].astype(jnp.float32) + total).astype(jnp.bfloat16)
+            middle[here, :] = mid
+            both[there, :] = scaled_rows(mid.astype(jnp.float32), gain_mlp[...])
+
+        spread(1, i)
 
     def activate(ranges):
         @pl.loop(0, whole)
@@ -611,71 +640,63 @@
 
     def expand(far, i=None):
         gathered(3)
-        if far:
-            arrived(1, 1, i)
-            activate(
-                [
-                    pl.ds(
-                        pl.multiple_of((side_of(1) * 2 + of) * rows + starts[i], 16), splits[i]
-                    )
-                    for of in (0, 1)
-                ]
-            )
-        else:
-            for part_index in range(len(splits)):
-                arrived(1, 0, part_index)
-            activate([tokens(0)])
+        activate(spans(1, far, i))
+
+    def drain():
+        for s in range(2 * len(fulls)):
+            ga.drain(s)
+        for i in range(len(splits)):
+            join_own(1, i, core).wait_send()
+            join_far(1, i, core).wait_send()
+            join_beside(1, i, 0).wait_send()
 
     def finish():
-        for block in range(blocks):
-            share(1, block).wait()
+        drain()
+        for rank in range(depth):
+            share(rank).wait()
         writes = []
-        for rank in range(depth):
-            origin = ga.near(rank)
-            for far in (1, 0):
-                block = ga.block(far, origin)
-                cols = block_cols(block)
-                give(1, block).wait_recv()
-                total = part[:, cols].astype(jnp.float32) + got[:, cols].astype(jnp.float32)
-                total = total + far_in[:, cols].astype(jnp.float32)
-                middle[:, cols] = (middle[:, cols].astype(jnp.float32) + total).astype(
+        for i in range(len(splits)):
+            here = part_rows(i)
+            for rank in range(depth):
+                cols = wide(rank)
+                give(rank, i).wait_recv()
+                total = part[here, cols].astype(jnp.float32) + got[here, cols].astype(jnp.float32)
+                total = total + far_in[here, cols].astype(jnp.float32)
+                middle[here, cols] = (middle[here, cols].astype(jnp.float32) + total).astype(
                     jnp.bfloat16
                 )
                 write = pltpu.make_async_copy(
-                    middle.at[:, cols], out.at[:, cols], out_sem.at[block]
+                    middle.at[here, cols], out.at[here, cols], load_sem.at[len(writes)]
                 )
                 write.start()
                 writes.append(write)
+        for rank in range(depth):
+            for i in range(len(splits)):
+                swap_far(rank, i).wait_send()
+                give(rank, i).wait_send()
         for write in writes:
             write.wait()
 
     order = [
-        (h, 2, 0), (h, 0, 0), (cross, 3), (cross, 1), (norm_mix,), (cross, 5), (h, 3, 0),
-        (h, 2, 1), (h, 1, 0), (h, 2, 2), (h, 1, 1), (h, 2, 3), (h, 3, 1), (cross, 9), (h, 0, 1),
-        (h, 3, 2), (h, 0, 2), (pass_on, 0, 0), (h, 4, 0), (h, 3, 3), (h, 1, 2), (h, 1, 3),
-        (h, 0, 3), (h, 6, 0), (pass_on, 0, 1), (values_of, 0), (h, 5, 0), (cross, 7),
-        (values_of, 1), (h, 4, 1), (pairs_of, 1), (retain, 1), (h, 5, 1), (far_rank, 0, 0),
-        (h, 4, 2), (pairs_of, 0), (h, 5, 2), (far_rank, 0, 1), (h, 6, 1), (h, 4, 3), (retain, 0),
-        (h, 5, 3), (far_rank, 0, 2), (h, 7, 0), (far_rank, 0, 3), (h, 6, 2), (own_rank, 0, 3),
-        (h, 7, 1), (own_rank, 0, 2), (own_rank, 0, 1), (own_rank, 0, 0), (h, 9, 0), (norm_mlp,),
-        (h, 6, 3), (h, 7, 2), (h, 7, 3), (h, 9, 1), (h, 8, 0), (pass_on, 1, 0), (h, 8, 1),
-        (h, 9, 2), (expand, 1, 0), (pass_on, 1, 1), (h, 8, 2), (h, 9, 3), (expand, 1, 1),
-        (far_rank, 1, 1), (far_rank, 1, 0), (expand, 0), (h, 8, 3), (own_rank, 1, 1),
-        (far_rank, 1, 2), (own_rank, 1, 0), (own_rank, 1, 2), (far_rank, 1, 3), (own_rank, 1, 3),
-        (finish,),
+        (cross, 1), (h, 0, 0), (h, 2, 0), (cross, 3), (norm_mix,), (h, 1, 0), (h, 0, 1),
+        (h, 1, 1), (h, 2, 1), (h, 1, 2), (h, 0, 2), (cross, 5), (h, 2, 2), (h, 1, 3), (h, 3, 0),
+        (h, 4, 0), (h, 0, 3), (h, 3, 1), (h, 2, 3), (pass_on, 0, 0), (cross, 9), (pairs_of, 1, 0),
+        (h, 3, 2), (h, 3, 3), (h, 4, 1), (pairs_of, 0), (cross, 7), (h, 4, 2), (pass_on, 0, 1),
+        (h, 5, 0), (pairs_of, 1, 1), (values_of, 1, 1), (values_of, 1, 0), (weigh, 1), (h, 5, 1),
+        (h, 4, 3), (retain, 1), (h, 6, 0), (far_rank, 0, 0, 1), (h, 5, 2), (far_rank, 0, 1, 0),
+        (h, 7, 0), (weigh, 0), (values_of, 0), (far_rank, 0, 2, 0), (h, 5, 3),
+        (far_rank, 0, 0, 0), (h, 6, 1), (retain, 0), (far_rank, 0, 3, 0), (far_rank, 0, 2, 1),
+        (h, 7, 1), (own_rank, 0, 0), (own_rank, 0, 1), (own_rank, 0, 2), (far_rank, 0, 3, 1),
+        (far_rank, 0, 1, 1), (own_rank, 0, 3), (h, 6, 2), (norm_mlp, 0), (h, 7, 2), (h, 6, 3),
+        (h, 8, 0), (h, 7, 3), (norm_mlp, 1), (h, 9, 0), (h, 8, 1), (pass_on, 1, 0), (h, 9, 1),
+        (expand, 1, 0), (h, 8, 2), (far_rank, 1, 0, 0), (pass_on, 1, 1), (h, 9, 2),
+        (far_rank, 1, 1, 0), (expand, 1, 1), (far_rank, 1, 0, 1), (far_rank, 1, 2, 0), (h, 8, 3),
+        (far_rank, 1, 1, 1), (h, 9, 3), (far_rank, 1, 2, 1), (expand, 0), (far_rank, 1, 3, 0),
+        (far_rank, 1, 3, 1), (own_rank, 1, 0), (own_rank, 1, 1), (own_rank, 1, 3),
+        (own_rank, 1, 2), (finish,),
     ]
     for job, *given in order:
         job(*given)
-    for s in range(2 * len(fulls)):
-        ga.drain(s)
-    for layer in (0, 1):
-        for i in range(len(splits)):
-            join_own(layer, i, core).wait_send()
-            join_far(layer, i, core).wait_send()
-            join_beside(layer, i, 0).wait_send()
-    for block in range(blocks):
-        swap_far(1, block).wait_send()
-        give(1, block).wait_send()
 
 
 def rotation_tables(length_total, half_width):
@@ -705,7 +726,7 @@
     fulls = []
     for (r, c), axis in zip(others, (0, 0, 1, 0, 1)):
         fulls.append((r * size, c) if axis == 0 else (r, c * size))
-    along = [shard // 2, shard // 2, DV // 2, shard // 16 * 9 // 16 * 16, units // 2 // 2]
+    along = [shard // 2, shard // 16 * 9 // 16 * 16, DV // 16 * 18 // 32 * 16, shard // 2, units // 2 // 16 * 30 // 44 * 16]
     splits = (2 * rows // 3, rows // 3)
     cosine, sine = rotation_tables(2 * rows, DK // 2)
     far = pl.BlockSpec(memory_space=pl.ANY)
@@ -713,7 +734,7 @@
     vm = pltpu.VMEM
     dma = pltpu.SemaphoreType.DMA
     slices = 2 * len(fulls)
-    peers = 2 * len(splits) + 2 * size
+    peers = 2 * len(splits) + (1 + len(splits)) * depth
     args = [a[None, :] if a.ndim == 1 else a for a in args]
     return pl.pallas_call(
         functools.partial(layer_kernel, depth, splits, along),
@@ -744,16 +765,15 @@
         + [vm((rows, width), bf)] * 9
         + [vm((BLOCK, BLOCK), f32)] * 3
         + [
-            dma((slices, 3, depth)),
-            dma((slices, 2, depth)),
+            dma((slices, 2 * depth + 1)),
+            dma((slices, 2 * depth)),
             dma((len(fulls),)),
             dma((len(fulls),)),
             dma((22,)),
-            dma((2, peers)),
-            dma((2, peers)),
-            dma((2, len(splits) + size)),
-            dma((2, len(splits) + size)),
-            dma((size,)),
+            dma((peers,)),
+            dma((peers,)),
+            dma((len(splits) * (1 + depth),)),
+            dma((len(splits) * (1 + depth),)),
         ],
         compiler_params=pltpu.CompilerParams(
             collective_id=0, has_side_effects=True, vmem_limit_bytes=67043328

time: 181 us -> 169 us (0.934)
  Pallas kernels: 178 us -> 166 us
    pallas_call x1, Pallas kernels: 178 us -> 166 us  [layer(): pl.pallas_call(functools.partial(layer_kernel, depth, splits, along), out...]
where the time goes in v4:
time: 169 us
  Pallas kernels  166 us (98%)
  local copies, waits for them, and re-layouts  2.73 us (2%)
    pallas_call x1, Pallas kernels, layer(): pl.pallas_call(functools.partial(layer_kernel, depth, splits, along), out...  166 us

profile of v4, /device:TPU:0, one launch (start us, length us, event | category | flops | bytes accessed | tf_op | source)
XLA Modules:
  0.0 168.7 jit_solution(2139878435464763678)
XLA Ops:
  0.0 165.9 %shard_map.127 = bf16[384,2048]{1,0:T(8,128)(2,1)} custom-call(bf16[384,2048]{1,0:T(8,128)(2,1)} %refs_0_.1, f32[1,2048]{1,0:T(1,128)} %bitcast.3, bf16[256,512]{1,0:T(8,128)(2,1)} %refs_2_.1, bf16[256,512]{1,0:T(8,128)(2,1)} %refs_3_.1, bf16[256,1024]{1,0:T(8,128)(2,1)} %refs_4_.1, f32[1,1024]{1,0:T(1,128)} %bitcast.5, bf16[1024,256]{1,0:T(8,128)(2,1)} %refs_6_.1, ...), custom_call_target="tpu_custom_call" | custom-call | tf_op jit(solution)/shard_map/pallas_call | solution.py:739
  166.0 2.7 %copy.15 = bf16[384,2048]{1,0:T(8,128)(2,1)} copy(bf16[384,2048]{1,0:T(8,128)(2,1)} %shard_map.127) | data formatting | bytes 3145728

commit v5 on v4

--- a/solution.py
+++ b/solution.py
@@ -678,22 +678,22 @@
             write.wait()
 
     order = [
-        (cross, 1), (h, 0, 0), (h, 2, 0), (cross, 3), (norm_mix,), (h, 1, 0), (h, 0, 1),
-        (h, 1, 1), (h, 2, 1), (h, 1, 2), (h, 0, 2), (cross, 5), (h, 2, 2), (h, 1, 3), (h, 3, 0),
-        (h, 4, 0), (h, 0, 3), (h, 3, 1), (h, 2, 3), (pass_on, 0, 0), (cross, 9), (pairs_of, 1, 0),
-        (h, 3, 2), (h, 3, 3), (h, 4, 1), (pairs_of, 0), (cross, 7), (h, 4, 2), (pass_on, 0, 1),
-        (h, 5, 0), (pairs_of, 1, 1), (values_of, 1, 1), (values_of, 1, 0), (weigh, 1), (h, 5, 1),
-        (h, 4, 3), (retain, 1), (h, 6, 0), (far_rank, 0, 0, 1), (h, 5, 2), (far_rank, 0, 1, 0),
-        (h, 7, 0), (weigh, 0), (values_of, 0), (far_rank, 0, 2, 0), (h, 5, 3),
-        (far_rank, 0, 0, 0), (h, 6, 1), (retain, 0), (far_rank, 0, 3, 0), (far_rank, 0, 2, 1),
-        (h, 7, 1), (own_rank, 0, 0), (own_rank, 0, 1), (own_rank, 0, 2), (far_rank, 0, 3, 1),
-        (far_rank, 0, 1, 1), (own_rank, 0, 3), (h, 6, 2), (norm_mlp, 0), (h, 7, 2), (h, 6, 3),
-        (h, 8, 0), (h, 7, 3), (norm_mlp, 1), (h, 9, 0), (h, 8, 1), (pass_on, 1, 0), (h, 9, 1),
-        (expand, 1, 0), (h, 8, 2), (far_rank, 1, 0, 0), (pass_on, 1, 1), (h, 9, 2),
-        (far_rank, 1, 1, 0), (expand, 1, 1), (far_rank, 1, 0, 1), (far_rank, 1, 2, 0), (h, 8, 3),
-        (far_rank, 1, 1, 1), (h, 9, 3), (far_rank, 1, 2, 1), (expand, 0), (far_rank, 1, 3, 0),
-        (far_rank, 1, 3, 1), (own_rank, 1, 0), (own_rank, 1, 1), (own_rank, 1, 3),
-        (own_rank, 1, 2), (finish,),
+        (h, 2, 0), (cross, 1), (h, 0, 0), (cross, 3), (norm_mix,), (cross, 5), (h, 1, 0),
+        (h, 2, 1), (h, 0, 1), (h, 1, 1), (h, 2, 2), (h, 0, 2), (cross, 7), (h, 3, 0), (h, 1, 2),
+        (cross, 9), (h, 0, 3), (h, 1, 3), (h, 4, 0), (h, 3, 1), (h, 3, 2), (pass_on, 0, 0),
+        (h, 2, 3), (h, 6, 0), (h, 3, 3), (pairs_of, 1, 0), (pass_on, 0, 1), (h, 5, 0),
+        (pairs_of, 1, 1), (h, 4, 1), (weigh, 1), (values_of, 1, 0), (values_of, 1, 1), (h, 5, 1),
+        (retain, 1), (h, 4, 2), (far_rank, 0, 0, 0), (h, 5, 2), (values_of, 0), (h, 7, 0),
+        (h, 4, 3), (far_rank, 0, 0, 1), (h, 5, 3), (far_rank, 0, 1, 0), (far_rank, 0, 1, 1),
+        (h, 6, 1), (far_rank, 0, 2, 0), (pairs_of, 0), (h, 7, 1), (weigh, 0), (retain, 0),
+        (far_rank, 0, 3, 0), (far_rank, 0, 2, 1), (own_rank, 0, 3), (own_rank, 0, 2),
+        (far_rank, 0, 3, 1), (h, 6, 2), (own_rank, 0, 1), (own_rank, 0, 0), (norm_mlp, 0),
+        (h, 7, 2), (h, 6, 3), (h, 8, 0), (h, 7, 3), (norm_mlp, 1), (h, 9, 0), (pass_on, 1, 0),
+        (h, 8, 1), (h, 9, 1), (expand, 1, 0), (h, 8, 2), (far_rank, 1, 0, 0), (pass_on, 1, 1),
+        (far_rank, 1, 1, 0), (h, 9, 2), (expand, 1, 1), (far_rank, 1, 0, 1), (far_rank, 1, 1, 1),
+        (h, 8, 3), (h, 9, 3), (far_rank, 1, 2, 1), (far_rank, 1, 2, 0), (expand, 0),
+        (far_rank, 1, 3, 0), (far_rank, 1, 3, 1), (own_rank, 1, 0), (own_rank, 1, 2),
+        (own_rank, 1, 1), (own_rank, 1, 3), (finish,),
     ]
     for job, *given in order:
         job(*given)
@@ -726,7 +726,7 @@
     fulls = []
     for (r, c), axis in zip(others, (0, 0, 1, 0, 1)):
         fulls.append((r * size, c) if axis == 0 else (r, c * size))
-    along = [shard // 2, shard // 16 * 9 // 16 * 16, DV // 16 * 18 // 32 * 16, shard // 2, units // 2 // 16 * 30 // 44 * 16]
+    along = [shard // 2, shard // 2, DV // 2, shard // 16 * 9 // 16 * 16, units // 2 // 16 * 27 // 44 * 16]
     splits = (2 * rows // 3, rows // 3)
     cosine, sine = rotation_tables(2 * rows, DK // 2)
     far = pl.BlockSpec(memory_space=pl.ANY)

time: 169 us -> 167 us (0.988)
  no operation moved by 1% of the time
where the time goes in v5:
time: 167 us
  Pallas kernels  165 us (99%)
  local copies, waits for them, and re-layouts  2.73 us (2%)
    pallas_call x1, Pallas kernels, layer(): pl.pallas_call(functools.partial(layer_kernel, depth, splits, along), out...  165 us

profile of v5, /device:TPU:0, one launch (start us, length us, event | category | flops | bytes accessed | tf_op | source)
XLA Modules:
  0.0 167.3 jit_solution(2895467792836306365)
XLA Ops:
  0.0 164.6 %shard_map.127 = bf16[384,2048]{1,0:T(8,128)(2,1)} custom-call(bf16[384,2048]{1,0:T(8,128)(2,1)} %refs_0_.1, f32[1,2048]{1,0:T(1,128)} %bitcast.3, bf16[256,512]{1,0:T(8,128)(2,1)} %refs_2_.1, bf16[256,512]{1,0:T(8,128)(2,1)} %refs_3_.1, bf16[256,1024]{1,0:T(8,128)(2,1)} %refs_4_.1, f32[1,1024]{1,0:T(1,128)} %bitcast.5, bf16[1024,256]{1,0:T(8,128)(2,1)} %refs_6_.1, ...), custom_call_target="tpu_custom_call" | custom-call | tf_op jit(solution)/shard_map/pallas_call | solution.py:739
  164.6 2.7 %copy.15 = bf16[384,2048]{1,0:T(8,128)(2,1)} copy(bf16[384,2048]{1,0:T(8,128)(2,1)} %shard_map.127) | data formatting | bytes 3145728
